TPU v7x, 512 devices: a whole 4x4x16 slice. The times are simulated.
512 devices in a mesh: sp: 16 (over z), dp: 32 (over y, x, core).
Axes of the slice: x: 4, y: 4, z: 16, core: 2. Of those that a mesh axis runs over, the one named last changes fastest.
Arguments:
- cotangent: bfloat16 [32, 2048, 2048], P('dp', 'sp'), may hold values from -6 to 6
- unit_pre: bfloat16 [32, 2048, 2048], P('dp', None, 'sp'), may hold values from -6 to 6
- gate_pre: bfloat16 [32, 2048, 2048], P('dp', None, 'sp'), may hold values from -15 to 15
- out_weight: bfloat16 [2048, 2048], P('dp', 'sp'), may hold values from -0.125 to 0.125
- mix_weight: bfloat16 [8, 128, 128], replicated, may hold values from -0.5 to 0.5
- mix_bias: bfloat16 [8, 128], replicated, may hold values from 0.099609375 to 1.8984375
- norm_gain: bfloat16 [2048], P('sp'), may hold values from 0.099609375 to 1.8984375
- norm_shift: bfloat16 [2048], P('sp'), may hold values from -3 to 3
Outputs:
- unit_grad: bfloat16 [32, 2048, 2048], P('dp', None, 'sp')
- gate_grad: bfloat16 [32, 2048, 2048], P('dp', None, 'sp')
- out_weight_grad: float32 [2048, 2048], P('dp', 'sp')
- mix_weight_grad: float32 [8, 128, 128], replicated
- mix_bias_grad: float32 [8, 128], replicated
- gain_grad: float32 [2048], P('sp')
- shift_grad: float32 [2048], P('sp')
All inputs are finite; a program needn't handle non-finite values.
Results may differ from a plain program's by a relative error of at most 0.015.
Values may be sent and summed in bfloat16 or wider, within the bound.
A program may use at most 64 MiB of HBM per device.

v0:
```python
import math

import jax
import jax.numpy as jnp
from jax import lax
from jax.sharding import Mesh
from jax.sharding import PartitionSpec as P

GW = 2048
GROUPS = 8
BLK = 128
DP = ("dp_0", "dp_1", "dp_2")


epsilon = 1e-05
tanh_coef = math.sqrt(2.0 / math.pi)


def sent_to_all(x, axis):
    devices = lax.axis_size(axis)
    return lax.all_to_all(jnp.broadcast_to(x[None], (devices, *x.shape)), axis, 0, 0, tiled=True)


def taken_together(x, axis):
    return sent_to_all(x, axis).sum(axis=0)


def packed_total(arrays, axis):
    flat, at, done = (jnp.concatenate([a.reshape(-1) for a in arrays]), 0, [])
    total = taken_together(flat, axis)
    for a in arrays:
        done.append(total[at : at + a.size].reshape(a.shape))
        at += a.size
    return tuple(done)


def joined_along(parts, dim):
    parts = jnp.moveaxis(parts, 0, dim)
    dims = parts.shape
    return parts.reshape(*dims[:dim], dims[dim] * dims[dim + 1], *dims[dim + 2 :])


def collect(x, axis, dim):
    parts = sent_to_all(x, axis)
    return joined_along(parts, dim)


def split_up(x, dim, devices):
    before, after = (x.shape[:dim], x.shape[dim + 1 :])
    return jnp.moveaxis(x.reshape(*before, devices, -1, *after), dim, 0)


def sum_at_owner(x, axis, dim):
    parts = split_up(x, dim, lax.axis_size(axis))
    arrived = lax.all_to_all(parts, axis, split_axis=0, concat_axis=0, tiled=True)
    return arrived.astype(jnp.float32).sum(axis=0)


def padded_to(lines, devices):
    spare = -len(lines) % devices
    return jnp.pad(lines, [(0, spare)] + [(0, 0)] * (lines.ndim - 1))


def gather_axes(x, axes, dim):
    far, near = axes
    first = sent_to_all(x, far)
    parts = jnp.swapaxes(sent_to_all(first, near), 0, 1)
    return joined_along(parts.reshape(-1, *x.shape), dim)


def sum_at_owner_2(x, axis, dim):
    devices = lax.axis_size(axis)
    parts = lax.all_to_all(split_up(x, dim, devices), axis, 0, 0, tiled=True)
    return jnp.sum(parts, axis=0)


def sum_in_two_steps(x, axes, dim):
    far, near = axes
    parts = split_up(x, dim, lax.axis_size(far))
    nearer = sum_at_owner_2(parts, near, dim + 1)
    arrived = lax.all_to_all(nearer, far, split_axis=0, concat_axis=0, tiled=True)
    return arrived.sum(axis=0)


def sum_by_parts(x, axes):
    padded = padded_to(x, lax.axis_size(axes[0]) * lax.axis_size(axes[1]))
    whole = gather_axes(sum_in_two_steps(padded, axes, 0), axes, 0)
    return lax.slice_in_dim(whole, 0, len(x)).reshape(x.shape)


def together(arrays, axis):
    ends = [0]
    for a in arrays:
        ends.append(ends[-1] + a.size)
    total = sum_by_parts(jnp.concatenate([a.ravel() for a in arrays]), axis)
    return tuple((total[b:e].reshape(a.shape) for a, b, e in zip(arrays, ends, ends[1:])))


def gelu_slope(values):
    inner = tanh_coef * (values + 0.044715 * values * values * values)
    hyper = jnp.tanh(inner)
    return 0.5 * (1.0 + hyper) + 0.5 * values * (1.0 - hyper * hyper) * tanh_coef * (
        1.0 + 3.0 * 0.044715 * values * values
    )


def local(cotangent, unit_pre, gate_pre, out_weight, mix_weight, mix_bias, norm_gain, norm_shift):
    seq_len = unit_pre.shape[1]
    channels = unit_pre.shape[2]
    group_dim = GW // GROUPS
    span_width = min(channels, group_dim)
    groups_here = channels // span_width
    blocks = seq_len // BLK
    group_start = lax.axis_index("sp") * channels // group_dim
    units = unit_pre[0].astype(jnp.float32)
    gates = gate_pre[0].astype(jnp.float32)
    unit_act = jax.nn.gelu(units)
    gate_act = jax.nn.gelu(gates)
    moments = packed_total(
        (jnp.sum(gate_act, axis=-1), jnp.sum(gate_act * gate_act, axis=-1)), "sp"
    )
    mean_val = moments[0] / GW
    var_val = moments[1] / GW - mean_val * mean_val
    rstd_val = lax.rsqrt(var_val + epsilon)
    centred = (gate_act - mean_val[:, None]) * rstd_val[:, None]
    gain_vec = norm_gain.astype(jnp.float32)
    normed = (centred * gain_vec + norm_shift.astype(jnp.float32)).astype(jnp.bfloat16)
    causal = jnp.arange(BLK)[:, None] >= jnp.arange(BLK)[None, :]
    local_weight = lax.dynamic_slice_in_dim(mix_weight, group_start, groups_here, 0)
    masked = jnp.where(causal[None], local_weight, jnp.zeros_like(local_weight))
    local_bias = lax.dynamic_slice_in_dim(mix_bias, group_start, groups_here, 0).astype(jnp.float32)
    normed_blocks = normed.reshape(blocks, BLK, groups_here, span_width)
    mixed = jnp.einsum("gts,nsgd->ntgd", masked, normed_blocks, preferred_element_type=jnp.float32)
    mixed = (mixed + local_bias.T[None, :, :, None]).reshape(seq_len, channels)
    gated = (unit_act * mixed).astype(jnp.bfloat16)
    weight_whole = collect(out_weight, DP, 0)
    dy_rows = lax.all_gather(cotangent, "sp", axis=1, tiled=True)[0]
    product = jnp.dot(dy_rows, weight_whole, preferred_element_type=jnp.float32)
    weight_part = lax.dot_general(
        dy_rows, gated, (((0,), (0,)), ((), ())), preferred_element_type=jnp.float32
    )
    token_count = lax.axis_size(DP) * seq_len
    norm_scale = 1.0 / math.sqrt(token_count)
    mix_scale = 1.0 / math.sqrt(token_count // BLK * group_dim)
    out_grad = sum_at_owner(weight_part.astype(jnp.bfloat16), DP, 0) * norm_scale
    unit_grad = (product * mixed * gelu_slope(units)).astype(jnp.bfloat16)
    mix_grad = product * unit_act
    mix_round = mix_grad.astype(jnp.bfloat16).reshape(blocks, BLK, groups_here, span_width)
    mix_term = jnp.einsum(
        "ntgd,nsgd->gts", mix_round, normed_blocks, preferred_element_type=jnp.float32
    )
    mix_term = jnp.where(causal[None], mix_term, jnp.float32(0.0))
    bias_term = jnp.sum(mix_grad.reshape(blocks, BLK, groups_here, span_width), axis=(0, 3)).T
    normed_grad = jnp.einsum(
        "gts,ntgd->nsgd", masked, mix_round, preferred_element_type=jnp.float32
    ).reshape(seq_len, channels)
    gain_term = jnp.sum(normed_grad * centred, axis=0)
    shift_term = jnp.sum(normed_grad, axis=0)
    scaled = normed_grad * gain_vec
    back_sums = packed_total((jnp.sum(scaled, axis=-1), jnp.sum(scaled * centred, axis=-1)), "sp")
    first_m = back_sums[0] / GW
    second_m = back_sums[1] / GW
    gate_grad = (
        rstd_val[:, None]
        * (scaled - first_m[:, None] - centred * second_m[:, None])
        * gelu_slope(gates)
    ).astype(jnp.bfloat16)
    empty_weight = jnp.zeros((GROUPS, BLK, BLK), jnp.float32)
    empty_bias = jnp.zeros((GROUPS, BLK), jnp.float32)
    full_weight = lax.dynamic_update_slice_in_dim(empty_weight, mix_term, group_start, 0)
    full_bias = lax.dynamic_update_slice_in_dim(empty_bias, bias_term, group_start, 0)
    full_weight, full_bias = together((full_weight, full_bias), (("sp", "dp_0"), ("dp_1", "dp_2")))
    gain_total, shift_total = packed_total((gain_term, shift_term), DP)
    return (
        unit_grad[None],
        gate_grad[None],
        out_grad,
        full_weight * mix_scale,
        full_bias * mix_scale,
        gain_total * norm_scale,
        shift_total * norm_scale,
    )


def solution(mesh):
    split = Mesh(mesh.devices.reshape(mesh.shape["sp"], 4, 4, 2), ("sp", "dp_0", "dp_1", "dp_2"))
    return jax.shard_map(
        local,
        mesh=split,
        in_specs=(
            P(DP, "sp", None),
            P(DP, None, "sp"),
            P(DP, None, "sp"),
            P(DP, "sp"),
            P(),
            P(),
            P("sp"),
            P("sp"),
        ),
        out_specs=(P(DP, None, "sp"), P(DP, None, "sp"), P(DP, "sp"), P(), P(), P("sp"), P("sp")),
        check_vma=False,
    )
```

profile of v0, /device:TPU:1, one launch (start us, length us, event | category | flops | bytes accessed | tf_op | source)
XLA Modules:
  0.0 283.7 jit_solution(611376720684969370)
XLA Ops:
  7.9 1.8 fusion.90
  10.6 15.7 %all-to-all-start.1 = ((f32[16,1,4096]{2,1,0:T(1,128)}), f32[16,1,4096]{2,1,0:T(1,128)S(1)}, u32[]{:S(2)}, u32[]{:S(2)}) async-start(f32[16,1,4096]{2,1,0:T(1,128)} %broadcast_in_dim.27), calls=%async_computation.1 | async-start | bytes 524288 | tf_op jit(solution)/shard_map/all_to_all | solution.py:21
  26.4 1.1 convert_element_type.100
  29.5 10.6 %all-to-all-done.1 = f32[16,1,4096]{2,1,0:T(1,128)S(1)} async-done(((f32[16,1,4096]{2,1,0:T(1,128)}), f32[16,1,4096]{2,1,0:T(1,128)S(1)}, u32[]{:S(2)}, u32[]{:S(2)}) %all-to-all-start.1) | async-done | bytes 262176 | tf_op jit(solution)/shard_map/all_to_all | solution.py:21
  40.1 1.6 broadcast_in_dim.26
  41.7 14.4 %all-to-all-start = ((bf16[32,64,128]{2,1,0:T(8,128)(2,1)}), bf16[32,64,128]{2,1,0:T(8,128)(2,1)S(1)}, u32[]{:S(2)}, u32[]{:S(2)}) async-start(bf16[32,64,128]{2,1,0:T(8,128)(2,1)} %broadcast_in_dim.26), calls=%async_computation | async-start | bytes 1048576 | tf_op jit(solution)/shard_map/all_to_all | solution.py:21
  56.4 1.7 add_convert_fusion
  58.1 2.7 fusion.50
  60.8 6.9 %all-to-all-done = bf16[32,64,128]{2,1,0:T(8,128)(2,1)S(1)} async-done(((bf16[32,64,128]{2,1,0:T(8,128)(2,1)}), bf16[32,64,128]{2,1,0:T(8,128)(2,1)S(1)}, u32[]{:S(2)}, u32[]{:S(2)}) %all-to-all-start) | async-done | bytes 524320 | tf_op jit(solution)/shard_map/all_to_all | solution.py:21
  67.6 59.1 %all-gather.2.cloned.1.call-done = bf16[1,2048,2048]{2,1,0:T(8,128)(2,1)} async-done(((bf16[1,128,2048]{2,1,0:T(8,128)(2,1)}), bf16[1,2048,2048]{2,1,0:T(8,128)(2,1)}) %all-gather.2.cloned.1.call-update) | async-done | bytes 8388624 | tf_op jit(solution)/shard_map/all_gather | solution.py:137
  126.7 7.7 %fusion.100 = (f32[2048]{0:T(1024)S(1)}, bf16[2048,128]{1,0:T(8,128)(2,1)}, bf16[2048,128]{1,0:T(8,128)(2,1)}) fusion(bf16[1,2048,128]{2,1,0:T(8,128)(2,1)S(1)} %copy-done.1, f32[1,16,128,128]{2,3,1,0:T(8,128)} %get-tuple-element.26, bf16[2048,128]{1,0:T(8,128)(2,1)S(1)} %bitcast.170, bf16[1,2048,2048]{2,1,0:T(8,128)(2,1)} %all-gather.2.cloned.1.call-done), kind=kOutput, calls=%fused_computation.126 | convolution fusion | flops 1082128384 | bytes 11542528 | tf_op jit(solution)/shard_map/dot_general | solution.py:138
  134.5 1.8 fusion.17
  137.1 1.1 copy.34
  138.2 4.8 %all-to-all-start.4 = ((f32[8,64,258]{2,1,0:T(8,128)}), f32[8,64,258]{2,1,0:T(8,128)S(1)}, u32[]{:S(2)}, u32[]{:S(2)}) async-start(f32[8,64,258]{2,1,0:T(8,128)} %copy.34), calls=%async_computation.4 | async-start | bytes 1572864 | tf_op jit(solution)/shard_map/all_to_all | solution.py:73
  143.0 2.7 fusion.85
  146.0 9.2 %all-to-all-done.4 = f32[8,64,258]{2,1,0:T(8,128)S(1)} async-done(((f32[8,64,258]{2,1,0:T(8,128)}), f32[8,64,258]{2,1,0:T(8,128)S(1)}, u32[]{:S(2)}, u32[]{:S(2)}) %all-to-all-start.4) | async-done | bytes 528416 | tf_op jit(solution)/shard_map/all_to_all | solution.py:73
  155.8 6.2 %all-to-all-start.8 = ((f32[32,1,256]{2,1,0:T(1,128)}), f32[32,1,256]{2,1,0:T(1,128)S(1)}, u32[]{:S(2)}, u32[]{:S(2)}) async-start(f32[32,1,256]{2,1,0:T(1,128)} %broadcast_in_dim.37), calls=%async_computation.8 | async-start | bytes 65536 | tf_op jit(solution)/shard_map/all_to_all | solution.py:21
  162.8 6.5 %all-to-all-done.8 = f32[32,1,256]{2,1,0:T(1,128)S(1)} async-done(((f32[32,1,256]{2,1,0:T(1,128)}), f32[32,1,256]{2,1,0:T(1,128)S(1)}, u32[]{:S(2)}, u32[]{:S(2)}) %all-to-all-start.8) | async-done | bytes 32800 | tf_op jit(solution)/shard_map/all_to_all | solution.py:21
  169.3 10.7 %all-to-all-start.5 = ((f32[64,1,258]{2,1,0:T(1,128)}), f32[64,1,258]{2,1,0:T(1,128)S(1)}, u32[]{:S(2)}, u32[]{:S(2)}) async-start(f32[64,1,258]{2,1,0:T(1,128)} %all_to_all.39), calls=%async_computation.5 | async-start | bytes 196608 | tf_op jit(solution)/shard_map/all_to_all | solution.py:81
  180.0 4.7 %fusion.7 = bf16[2048,128]{0,1:T(8,128)(2,1)S(1)} fusion(bf16[2048,128]{1,0:T(8,128)(2,1)S(1)} %bitcast.166, bf16[1,2048,2048]{2,1,0:T(8,128)(2,1)} %all-gather.2.cloned.1.call-done), kind=kOutput, calls=%fused_computation.17 | convolution fusion | flops 1074003968 | bytes 9437184 | tf_op jit(solution)/shard_map/dot_general | solution.py:139
  184.8 1.0 copy.33
  185.8 8.8 %all-to-all-done.5 = f32[64,1,258]{2,1,0:T(1,128)S(1)} async-done(((f32[64,1,258]{2,1,0:T(1,128)}), f32[64,1,258]{2,1,0:T(1,128)S(1)}, u32[]{:S(2)}, u32[]{:S(2)}) %all-to-all-start.5) | async-done | bytes 66080 | tf_op jit(solution)/shard_map/all_to_all | solution.py:81
  194.6 6.5 %all-to-all-start.3 = ((bf16[32,64,128]{2,1,0:T(8,128)(2,1)}), bf16[32,64,128]{2,1,0:T(8,128)(2,1)S(1)}, u32[]{:S(2)}, u32[]{:S(2)}) async-start(bf16[32,64,128]{2,1,0:T(8,128)(2,1)} %bitcast.27), calls=%async_computation.3 | async-start | bytes 1048576 | tf_op jit(solution)/shard_map/all_to_all | solution.py:55
  201.2 11.3 %all-to-all-done.3 = bf16[32,64,128]{2,1,0:T(8,128)(2,1)S(1)} async-done(((bf16[32,64,128]{2,1,0:T(8,128)(2,1)}), bf16[32,64,128]{2,1,0:T(8,128)(2,1)S(1)}, u32[]{:S(2)}, u32[]{:S(2)}) %all-to-all-start.3) | async-done | bytes 524320 | tf_op jit(solution)/shard_map/all_to_all | solution.py:55
  213.2 4.6 %all-to-all-start.6 = ((f32[64,1,258]{2,1,0:T(1,128)}), f32[64,1,258]{2,1,0:T(1,128)S(1)}, u32[]{:S(2)}, u32[]{:S(2)}) async-start(f32[64,1,258]{2,1,0:T(1,128)} %broadcast_in_dim.34), calls=%async_computation.6 | async-start | bytes 196608 | tf_op jit(solution)/shard_map/all_to_all | solution.py:21
  217.9 14.6 %all-to-all-done.6 = f32[64,1,258]{2,1,0:T(1,128)S(1)} async-done(((f32[64,1,258]{2,1,0:T(1,128)}), f32[64,1,258]{2,1,0:T(1,128)S(1)}, u32[]{:S(2)}, u32[]{:S(2)}) %all-to-all-start.6) | async-done | bytes 66080 | tf_op jit(solution)/shard_map/all_to_all | solution.py:21
  233.3 4.1 %all-to-all-start.2 = ((f32[16,1,4096]{2,1,0:T(1,128)}), f32[16,1,4096]{2,1,0:T(1,128)S(1)}, u32[]{:S(2)}, u32[]{:S(2)}) async-start(f32[16,1,4096]{2,1,0:T(1,128)} %broadcast_in_dim.30), calls=%async_computation.2 | async-start | bytes 524288 | tf_op jit(solution)/shard_map/all_to_all | solution.py:21
  238.7 11.4 %all-to-all-done.2 = f32[16,1,4096]{2,1,0:T(1,128)S(1)} async-done(((f32[16,1,4096]{2,1,0:T(1,128)}), f32[16,1,4096]{2,1,0:T(1,128)S(1)}, u32[]{:S(2)}, u32[]{:S(2)}) %all-to-all-start.2) | async-done | bytes 262176 | tf_op jit(solution)/shard_map/all_to_all | solution.py:21
  250.1 0.9 broadcast_in_dim.36
  251.1 10.8 %all-to-all-start.7 = ((f32[8,64,258]{2,1,0:T(8,128)}), f32[8,64,258]{2,1,0:T(8,128)S(1)}, u32[]{:S(2)}, u32[]{:S(2)}) async-start(f32[8,64,258]{2,1,0:T(8,128)} %broadcast_in_dim.36), calls=%async_computation.7 | async-start | bytes 1572864 | tf_op jit(solution)/shard_map/all_to_all | solution.py:21
  262.0 2.7 fusion.80
  264.7 9.3 %all-to-all-done.7 = f32[8,64,258]{2,1,0:T(8,128)S(1)} async-done(((f32[8,64,258]{2,1,0:T(8,128)}), f32[8,64,258]{2,1,0:T(8,128)S(1)}, u32[]{:S(2)}, u32[]{:S(2)}) %all-to-all-start.7) | async-done | bytes 528416 | tf_op jit(solution)/shard_map/all_to_all | solution.py:21
  (41 shorter events, 12.5 us)
Async XLA Ops:
  7.2 119.5 %copy-start.1 = (bf16[1,2048,128]{2,1,0:T(8,128)(2,1)S(1)}, bf16[1,2048,128]{2,1,0:T(8,128)(2,1)}, u32[]{:S(2)}) copy-start(bf16[1,2048,128]{2,1,0:T(8,128)(2,1)} %param.9) | copy-start | bytes 1572868
  7.2 119.5 %all-gather.2.cloned.1.call-start = ((), (), s32[]{:S(2)}) async-start(), calls=%async_computation.9 | async-start | bytes 8912896 | tf_op jit(solution)/shard_map/all_gather | solution.py:137
  10.6 29.5 %all-to-all-start.1 = ((f32[16,1,4096]{2,1,0:T(1,128)}), f32[16,1,4096]{2,1,0:T(1,128)S(1)}, u32[]{:S(2)}, u32[]{:S(2)}) async-start(f32[16,1,4096]{2,1,0:T(1,128)} %broadcast_in_dim.27), calls=%async_computation.1 | async-start | bytes 524288 | tf_op jit(solution)/shard_map/all_to_all | solution.py:21
  41.7 25.9 %all-to-all-start = ((bf16[32,64,128]{2,1,0:T(8,128)(2,1)}), bf16[32,64,128]{2,1,0:T(8,128)(2,1)S(1)}, u32[]{:S(2)}, u32[]{:S(2)}) async-start(bf16[32,64,128]{2,1,0:T(8,128)(2,1)} %broadcast_in_dim.26), calls=%async_computation | async-start | bytes 1048576 | tf_op jit(solution)/shard_map/all_to_all | solution.py:21
  138.2 17.0 %all-to-all-start.4 = ((f32[8,64,258]{2,1,0:T(8,128)}), f32[8,64,258]{2,1,0:T(8,128)S(1)}, u32[]{:S(2)}, u32[]{:S(2)}) async-start(f32[8,64,258]{2,1,0:T(8,128)} %copy.34), calls=%async_computation.4 | async-start | bytes 1572864 | tf_op jit(solution)/shard_map/all_to_all | solution.py:73
  155.8 13.5 %all-to-all-start.8 = ((f32[32,1,256]{2,1,0:T(1,128)}), f32[32,1,256]{2,1,0:T(1,128)S(1)}, u32[]{:S(2)}, u32[]{:S(2)}) async-start(f32[32,1,256]{2,1,0:T(1,128)} %broadcast_in_dim.37), calls=%async_computation.8 | async-start | bytes 65536 | tf_op jit(solution)/shard_map/all_to_all | solution.py:21
  169.3 25.4 %all-to-all-start.5 = ((f32[64,1,258]{2,1,0:T(1,128)}), f32[64,1,258]{2,1,0:T(1,128)S(1)}, u32[]{:S(2)}, u32[]{:S(2)}) async-start(f32[64,1,258]{2,1,0:T(1,128)} %all_to_all.39), calls=%async_computation.5 | async-start | bytes 196608 | tf_op jit(solution)/shard_map/all_to_all | solution.py:81
  180.0 82.0 %copy-start = (bf16[1,2048,128]{2,1,0:T(8,128)(2,1)S(1)}, bf16[1,2048,128]{2,1,0:T(8,128)(2,1)}, u32[]{:S(2)}) copy-start(bf16[1,2048,128]{2,1,0:T(8,128)(2,1)} %param.10) | copy-start | bytes 1572868
  194.6 17.9 %all-to-all-start.3 = ((bf16[32,64,128]{2,1,0:T(8,128)(2,1)}), bf16[32,64,128]{2,1,0:T(8,128)(2,1)S(1)}, u32[]{:S(2)}, u32[]{:S(2)}) async-start(bf16[32,64,128]{2,1,0:T(8,128)(2,1)} %bitcast.27), calls=%async_computation.3 | async-start | bytes 1048576 | tf_op jit(solution)/shard_map/all_to_all | solution.py:55
  213.2 19.2 %all-to-all-start.6 = ((f32[64,1,258]{2,1,0:T(1,128)}), f32[64,1,258]{2,1,0:T(1,128)S(1)}, u32[]{:S(2)}, u32[]{:S(2)}) async-start(f32[64,1,258]{2,1,0:T(1,128)} %broadcast_in_dim.34), calls=%async_computation.6 | async-start | bytes 196608 | tf_op jit(solution)/shard_map/all_to_all | solution.py:21
  233.3 16.8 %all-to-all-start.2 = ((f32[16,1,4096]{2,1,0:T(1,128)}), f32[16,1,4096]{2,1,0:T(1,128)S(1)}, u32[]{:S(2)}, u32[]{:S(2)}) async-start(f32[16,1,4096]{2,1,0:T(1,128)} %broadcast_in_dim.30), calls=%async_computation.2 | async-start | bytes 524288 | tf_op jit(solution)/shard_map/all_to_all | solution.py:21
  251.1 22.9 %all-to-all-start.7 = ((f32[8,64,258]{2,1,0:T(8,128)}), f32[8,64,258]{2,1,0:T(8,128)S(1)}, u32[]{:S(2)}, u32[]{:S(2)}) async-start(f32[8,64,258]{2,1,0:T(8,128)} %broadcast_in_dim.36), calls=%async_computation.7 | async-start | bytes 1572864 | tf_op jit(solution)/shard_map/all_to_all | solution.py:21
Sparse Core Ops, SparseCore 0:
  10.1 116.5 all-gather.1
where the time goes:
time: 285 us; the launch traced here: 284 us
  waiting for transfers between devices  148 us (52%)
  starting transfers between devices  77.9 us (27%)
  matrix products  19.6 us (7%)
  between operations  14.3 us (5%)
  other arithmetic  12.8 us (4%)
  local copies, waits for them, and re-layouts  10.8 us (4%)
    all_to_all x6, waiting for transfers between devices, sent_to_all(): lax.all_to_all(jnp.broadcast_to(x[None], (devices, *x.shape)), axis, 0, 0...  59.3 us
    all_gather x1, waiting for transfers between devices, local(): dy_rows = lax.all_gather(cotangent, 'sp', axis=1, tiled=True)[0]  59.1 us
    all_to_all x6, starting transfers between devices, sent_to_all(): lax.all_to_all(jnp.broadcast_to(x[None], (devices, *x.shape)), axis, 0, 0...  55.8 us
    all_to_all x1, waiting for transfers between devices, sum_at_owner(): lax.all_to_all(parts, axis, split_axis=0, concat_axis=0, tiled=True)  11.3 us
    all_to_all x1, starting transfers between devices, sum_in_two_steps(): lax.all_to_all(nearer, far, split_axis=0, concat_axis=0, tiled=True)  10.7 us
    all_to_all x1, waiting for transfers between devices, sum_at_owner_2(): parts = lax.all_to_all(split_up(x, dim, devices), axis, 0, 0, tiled=True)  9.2 us
    all_to_all x1, waiting for transfers between devices, sum_in_two_steps(): lax.all_to_all(nearer, far, split_axis=0, concat_axis=0, tiled=True)  8.85 us
    dot_general x1, matrix products, local(): product = jnp.dot(dy_rows, weight_whole, preferred_element_type=jnp.float32)  7.68 us
  transfers between devices with their start and end apart: 10, of which 10 were waited for; matrix products, arithmetic and copies ran while one was open for 9% of the time, Pallas kernels for 0%

commit v1 on v0

v1 whole, which is shorter than its diff:
```python
import math

import jax
import jax.numpy as jnp
from jax import lax
from jax.sharding import PartitionSpec as P

GW = 2048
GROUPS = 8
BLK = 128

epsilon = 1e-05
tanh_coef = math.sqrt(2.0 / math.pi)


def sum_over(x, axis):
    devices = lax.axis_size(axis)
    copies = jnp.broadcast_to(x[None], (devices, *x.shape))
    return lax.all_to_all(copies, axis, 0, 0, tiled=True).sum(axis=0)


def gelu_slope(values):
    inner = tanh_coef * (values + 0.044715 * values * values * values)
    hyper = jnp.tanh(inner)
    return 0.5 * (1.0 + hyper) + 0.5 * values * (1.0 - hyper * hyper) * tanh_coef * (
        1.0 + 3.0 * 0.044715 * values * values
    )


def local(cotangent, unit_pre, gate_pre, out_weight, mix_weight, mix_bias, norm_gain, norm_shift):
    seq_len = unit_pre.shape[1]
    channels = unit_pre.shape[2]
    group_dim = GW // GROUPS
    blocks = seq_len // BLK
    sp_size = lax.axis_size("sp")
    sp_at = lax.axis_index("sp")
    group = sp_at * channels // group_dim
    weight_rows = lax.all_gather(out_weight, "sp", axis=1, tiled=True)
    weight_whole = lax.all_gather(weight_rows, "dp", axis=0, tiled=True)
    units = unit_pre[0].astype(jnp.float32)
    gates = gate_pre[0].astype(jnp.float32)
    unit_act = jax.nn.gelu(units)
    gate_act = jax.nn.gelu(gates)
    moments = sum_over(
        jnp.stack([jnp.sum(gate_act, axis=-1), jnp.sum(gate_act * gate_act, axis=-1)]), "sp"
    )
    mean_val = moments[0] / GW
    var_val = moments[1] / GW - mean_val * mean_val
    rstd_val = lax.rsqrt(var_val + epsilon)
    centred = (gate_act - mean_val[:, None]) * rstd_val[:, None]
    gain_vec = norm_gain.astype(jnp.float32)
    normed = (centred * gain_vec + norm_shift.astype(jnp.float32)).astype(jnp.bfloat16)
    causal = jnp.arange(BLK)[:, None] >= jnp.arange(BLK)[None, :]
    local_weight = lax.dynamic_index_in_dim(mix_weight, group, 0, keepdims=False)
    masked = jnp.where(causal, local_weight, jnp.zeros_like(local_weight))
    local_bias = lax.dynamic_index_in_dim(mix_bias, group, 0, keepdims=False).astype(jnp.float32)
    normed_blocks = normed.reshape(blocks, BLK, channels)
    mixed = jnp.einsum("ts,nsd->ntd", masked, normed_blocks, preferred_element_type=jnp.float32)
    mixed = (mixed + local_bias[None, :, None]).reshape(seq_len, channels)
    gated = (unit_act * mixed).astype(jnp.bfloat16)
    gated_rows = lax.all_to_all(gated, "sp", split_axis=0, concat_axis=1, tiled=True)
    head_rows = jnp.dot(cotangent[0], weight_whole, preferred_element_type=jnp.float32)
    head = lax.all_to_all(
        head_rows.astype(jnp.bfloat16), "sp", split_axis=1, concat_axis=0, tiled=True
    ).astype(jnp.float32)
    weight_part = lax.dot_general(
        cotangent[0], gated_rows, (((0,), (0,)), ((), ())), preferred_element_type=jnp.float32
    ).astype(jnp.bfloat16)
    token_count = lax.axis_size("dp") * seq_len
    norm_scale = 1.0 / math.sqrt(token_count)
    mix_scale = 1.0 / math.sqrt(token_count // BLK * group_dim)
    plane_sum = lax.psum_scatter(weight_part, "dp", scatter_dimension=0, tiled=True)
    plane_parts = jnp.moveaxis(plane_sum.reshape(plane_sum.shape[0], sp_size, channels), 1, 0)
    arrived = lax.all_to_all(plane_parts, "sp", split_axis=0, concat_axis=0, tiled=True)
    out_grad = arrived.astype(jnp.float32).sum(axis=0) * norm_scale
    unit_grad = (head * mixed * gelu_slope(units)).astype(jnp.bfloat16)
    mix_grad = head * unit_act
    mix_round = mix_grad.astype(jnp.bfloat16).reshape(blocks, BLK, channels)
    mix_term = jnp.einsum("ntd,nsd->ts", mix_round, normed_blocks, preferred_element_type=jnp.float32)
    mix_term = jnp.where(causal, mix_term, jnp.float32(0.0))
    bias_term = jnp.sum(mix_grad.reshape(blocks, BLK, channels), axis=(0, 2))
    normed_grad = jnp.einsum(
        "ts,ntd->nsd", masked, mix_round, preferred_element_type=jnp.float32
    ).reshape(seq_len, channels)
    gain_term = jnp.sum(normed_grad * centred, axis=0)
    shift_term = jnp.sum(normed_grad, axis=0)
    scaled = normed_grad * gain_vec
    back_sums = sum_over(
        jnp.stack([jnp.sum(scaled, axis=-1), jnp.sum(scaled * centred, axis=-1)]), "sp"
    )
    first_m = back_sums[0] / GW
    second_m = back_sums[1] / GW
    gate_grad = (
        rstd_val[:, None]
        * (scaled - first_m[:, None] - centred * second_m[:, None])
        * gelu_slope(gates)
    ).astype(jnp.bfloat16)
    group_hot = (jnp.arange(GROUPS) == group).astype(jnp.float32)
    own_hot = (jnp.arange(sp_size) == sp_at).astype(jnp.float32)
    packed = jnp.concatenate(
        [
            (group_hot[:, None, None] * mix_term).reshape(GROUPS * BLK, BLK),
            group_hot[:, None] * bias_term,
            own_hot[:, None] * gain_term,
            own_hot[:, None] * shift_term,
        ]
    )
    total = lax.psum(packed, ("sp", "dp"))
    top = GROUPS * BLK
    weight_total = total[:top].reshape(GROUPS, BLK, BLK)
    bias_total = total[top : top + GROUPS]
    tail = total[top + GROUPS :]
    gain_total = lax.dynamic_index_in_dim(tail, sp_at, 0, keepdims=False)
    shift_total = lax.dynamic_index_in_dim(tail, sp_size + sp_at, 0, keepdims=False)
    return (
        unit_grad[None],
        gate_grad[None],
        out_grad,
        weight_total * mix_scale,
        bias_total * mix_scale,
        gain_total * norm_scale,
        shift_total * norm_scale,
    )


def solution(mesh):
    return jax.shard_map(
        local,
        mesh=mesh,
        in_specs=(
            P("dp", "sp", None),
            P("dp", None, "sp"),
            P("dp", None, "sp"),
            P("dp", "sp"),
            P(),
            P(),
            P("sp"),
            P("sp"),
        ),
        out_specs=(P("dp", None, "sp"), P("dp", None, "sp"), P("dp", "sp"), P(), P(), P("sp"), P("sp")),
        check_vma=False,
    )
```

time: 285 us -> 830 us (2.91)
  waiting for transfers between devices: 148 us -> 670 us
  blocking collectives: 0 us -> 33.5 us
  starting transfers between devices: 77.9 us -> 53.6 us
  local copies, waits for them, and re-layouts: 10.8 us -> 19.8 us
    psum x0 -> x1, waiting for transfers between devices: none -> 430 us  [local(): total = lax.psum(packed, ('sp', 'dp'))]
    unnamed x1 -> x4, waiting for transfers between devices: 0.68 us -> 115 us
    all_gather x0 -> x1, blocking collectives: none -> 33.5 us  [local(): weight_rows = lax.all_gather(out_weight, 'sp', axis=1, tiled=True)]
    all_to_all x9 -> x5, waiting for transfers between devices: 88.6 us -> 62 us  [the longest x1 22.5 us: local(): lax.all_to_all(head_rows.astype(jnp.bfloat16), 'sp', split_axis=1, concat...]
    all_to_all x9 -> x5, starting transfers between devices: 77.8 us -> 53.5 us  [the longest x2 19.2 us: sum_over(): return lax.all_to_all(copies, axis, 0, 0, tiled=True).sum(axis=0)]
    unnamed x5 -> x18, local copies, waits for them, and re-layouts: 0.02 us -> 15.4 us
  transfers between devices with their start and end apart: 10 -> 8, of which waited for: 10 -> 7; matrix products, arithmetic and copies ran while one was open for 9% -> 5% of each run, Pallas kernels for 0% -> 0%
where the time goes in v1:
time: 830 us; the launch traced here: 823 us
  waiting for transfers between devices  670 us (81%)
  starting transfers between devices  53.6 us (6%)
  blocking collectives  33.5 us (4%)
  local copies, waits for them, and re-layouts  19.8 us (2%)
  matrix products  18.9 us (2%)
  between operations  14 us (2%)
  other arithmetic  12.7 us (2%)
    psum x1, waiting for transfers between devices, local(): total = lax.psum(packed, ('sp', 'dp'))  430 us
    unnamed x4, waiting for transfers between devices  115 us
    all_gather x1, waiting for transfers between devices, local(): weight_whole = lax.all_gather(weight_rows, 'dp', axis=0, tiled=True)  62.6 us
    all_gather x1, blocking collectives, local(): weight_rows = lax.all_gather(out_weight, 'sp', axis=1, tiled=True)  33.5 us
    all_to_all x1, waiting for transfers between devices, local(): lax.all_to_all(head_rows.astype(jnp.bfloat16), 'sp', split_axis=1, concat...  22.5 us
    all_to_all x2, starting transfers between devices, sum_over(): return lax.all_to_all(copies, axis, 0, 0, tiled=True).sum(axis=0)  19.2 us
    all_to_all x1, waiting for transfers between devices, local(): lax.all_to_all(gated, 'sp', split_axis=0, concat_axis=1, tiled=True)  18.9 us
  transfers between devices with their start and end apart: 8, of which 7 were waited for; matrix products, arithmetic and copies ran while one was open for 5% of the time, Pallas kernels for 0%

profile of v1, /device:TPU:1, one launch (start us, length us, event | category | flops | bytes accessed | tf_op | source)
XLA Modules:
  0.0 822.8 jit_solution(9951408123859522207)
XLA Ops:
  7.2 33.5 %all_gather.6 = bf16[64,2048]{1,0:T(8,128)(2,1)} all-gather(bf16[64,128]{1,0:T(8,128)(2,1)} %param.11), channel_id=1, replica_groups=mesh['sp'=16,'dp'=32] {'sp'}, dimensions={1}, use_global_device_ids=true | all-gather | bytes 278528 | tf_op jit(solution)/shard_map/all_gather | solution.py:38
  40.7 1.8 fusion.58
  42.5 0.8 broadcast_in_dim.11
  43.3 6.3 all-to-all-start.1
  49.6 62.6 %all-gather.2.cloned.1.call-done = bf16[2048,2048]{1,0:T(8,128)(2,1)} async-done(((bf16[64,2048]{1,0:T(8,128)(2,1)}), bf16[2048,2048]{1,0:T(8,128)(2,1)}) %all-gather.2.cloned.1.call-update) | async-done | bytes 8388624 | tf_op jit(solution)/shard_map/all_gather | solution.py:39
  112.2 4.6 fusion.5
  116.9 0.9 copy.53
  117.8 12.0 %all-to-all-start = ((bf16[128,16,128]{2,0,1:T(8,128)(2,1)}), bf16[128,16,128]{2,0,1:T(8,128)(2,1)S(1)}, u32[]{:S(2)}, u32[]{:S(2)}) async-start(bf16[128,16,128]{2,0,1:T(8,128)(2,1)} %bitcast.135), calls=%async_computation | async-start | bytes 1048576 | tf_op jit(solution)/shard_map/all_to_all | solution.py:63
  130.0 22.5 %all-to-all-done = bf16[128,16,128]{2,0,1:T(8,128)(2,1)S(1)} async-done(((bf16[128,16,128]{2,0,1:T(8,128)(2,1)}), bf16[128,16,128]{2,0,1:T(8,128)(2,1)S(1)}, u32[]{:S(2)}, u32[]{:S(2)}) %all-to-all-start) | async-done | bytes 524320 | tf_op jit(solution)/shard_map/all_to_all | solution.py:63
  153.0 1.0 copy-done.3
  154.0 3.3 fusion.56
  157.3 0.8 broadcast_in_dim.15
  158.1 12.9 %all-to-all-start.2 = ((f32[16,2,2048]{2,1,0:T(2,128)}), f32[16,2,2048]{2,1,0:T(2,128)S(1)}, u32[]{:S(2)}, u32[]{:S(2)}) async-start(f32[16,2,2048]{2,1,0:T(2,128)} %broadcast_in_dim.15), calls=%async_computation.2 | async-start | bytes 524288 | tf_op jit(solution)/shard_map/all_to_all | solution.py:19
  171.7 13.1 %all-to-all-done.2 = f32[16,2,2048]{2,1,0:T(2,128)S(1)} async-done(((f32[16,2,2048]{2,1,0:T(2,128)}), f32[16,2,2048]{2,1,0:T(2,128)S(1)}, u32[]{:S(2)}, u32[]{:S(2)}) %all-to-all-start.2) | async-done | bytes 262176 | tf_op jit(solution)/shard_map/all_to_all | solution.py:19
  184.9 2.8 fusion.51
  187.7 3.0 multiply_convert_fusion
  190.7 10.3 %all-to-all-start.3 = ((bf16[16,128,128]{2,1,0:T(8,128)(2,1)}), bf16[16,128,128]{2,1,0:T(8,128)(2,1)S(1)}, u32[]{:S(2)}, u32[]{:S(2)}) async-start(bf16[16,128,128]{2,1,0:T(8,128)(2,1)} %get-tuple-element.36), calls=%async_computation.3 | async-start | bytes 1048576 | tf_op jit(solution)/shard_map/all_to_all | solution.py:61
  201.4 2.5 fusion.6
  204.2 0.8 pad_maximum_fusion
  205.1 18.9 %all-to-all-done.3 = bf16[16,128,128]{2,1,0:T(8,128)(2,1)S(1)} async-done(((bf16[16,128,128]{2,1,0:T(8,128)(2,1)}), bf16[16,128,128]{2,1,0:T(8,128)(2,1)S(1)}, u32[]{:S(2)}, u32[]{:S(2)}) %all-to-all-start.3) | async-done | bytes 524320 | tf_op jit(solution)/shard_map/all_to_all | solution.py:61
  224.3 5.5 convert_bitcast_fusion
  229.8 12.4 %copy.42 = bf16[2048,2048]{1,0:T(8,128)(2,1)} copy(bf16[2048,2048]{0,1:T(8,128)(2,1)} %convert_bitcast_fusion) | data formatting | bytes 16777216
  242.2 430.2 %all-reduce.2.cloned.1.call-done = f32[1064,128]{1,0:T(8,128)} async-done(((f32[1064,128]{1,0:T(8,128)}), f32[1064,128]{1,0:T(8,128)}) %all-reduce.2.cloned.1.call-update) | async-done | bytes 544784 | tf_op jit(solution)/shard_map/psum | solution.py:108
  672.4 0.7 slice.34
  673.2 115.4 %reduce-scatter.4.cloned.1.call-done = bf16[64,2048]{1,0:T(8,128)(2,1)} async-done(((bf16[2048,2048]{1,0:T(8,128)(2,1)}), bf16[64,2048]{1,0:T(8,128)(2,1)}) %reduce-scatter.4.cloned.1.call-update) | async-done | bytes 262160
  788.6 1.2 copy.43
  789.8 0.9 copy.37
  790.7 12.0 %all-to-all-start.4 = ((bf16[16,64,128]{2,1,0:T(8,128)(2,1)}), bf16[16,64,128]{2,1,0:T(8,128)(2,1)S(1)}, u32[]{:S(2)}, u32[]{:S(2)}) async-start(bf16[16,64,128]{2,1,0:T(8,128)(2,1)} %bitcast.29), calls=%async_computation.4 | async-start | bytes 524288 | tf_op jit(solution)/shard_map/all_to_all | solution.py:74
  803.2 1.3 slice_multiply_fusion.5
  804.5 1.9 slice_multiply_fusion
  806.4 1.5 fusion.30
  807.9 7.5 all-to-all-done.4
  (44 shorter events, 4.0 us)
Async XLA Ops:
  7.2 105.0 %copy-start = (bf16[1,128,2048]{2,1,0:T(8,128)(2,1)S(1)}, bf16[1,128,2048]{2,1,0:T(8,128)(2,1)}, u32[]{:S(2)}) copy-start(bf16[1,128,2048]{2,1,0:T(8,128)(2,1)} %param.8) | copy-start | bytes 1572868
  7.2 105.0 %all-gather.2.cloned.1.call-start = ((), (), s32[]{:S(2)}) async-start(), calls=%async_computation.6 | async-start | bytes 8650752 | tf_op jit(solution)/shard_map/all_gather | solution.py:39
  43.3 74.5 %all-to-all-start.1 = ((f32[16,2,2048]{2,1,0:T(2,128)}), f32[16,2,2048]{2,1,0:T(2,128)S(1)}, u32[]{:S(2)}, u32[]{:S(2)}) async-start(f32[16,2,2048]{2,1,0:T(2,128)} %broadcast_in_dim.11), calls=%async_computation.1 | async-start | bytes 524288 | tf_op jit(solution)/shard_map/all_to_all | solution.py:19
  49.6 80.3 %copy-start.5 = (bf16[128]{0:T(256)(128)(2,1)S(1)}, bf16[128]{0:T(256)(128)(2,1)}, u32[]{:S(2)}) copy-start(bf16[128]{0:T(256)(128)(2,1)} %param.14) | copy-start | bytes 772
  49.6 102.9 %copy-start.2 = (bf16[1,2048,128]{2,1,0:T(8,128)(2,1)S(1)}, bf16[1,2048,128]{2,1,0:T(8,128)(2,1)}, u32[]{:S(2)}) copy-start(bf16[1,2048,128]{2,1,0:T(8,128)(2,1)} %param.9) | copy-start | bytes 1572868
  49.6 104.4 %copy-start.1 = (bf16[1,2048,128]{2,1,0:T(8,128)(2,1)S(1)}, bf16[1,2048,128]{2,1,0:T(8,128)(2,1)}, u32[]{:S(2)}) copy-start(bf16[1,2048,128]{2,1,0:T(8,128)(2,1)} %param.10) | copy-start | bytes 1572868
  116.9 54.2 %copy-start.6 = (bf16[128]{0:T(256)(128)(2,1)S(1)}, bf16[128]{0:T(256)(128)(2,1)}, u32[]{:S(2)}) copy-start(bf16[128]{0:T(256)(128)(2,1)} %param.15) | copy-start | bytes 772
  117.8 34.7 %all-to-all-start = ((bf16[128,16,128]{2,0,1:T(8,128)(2,1)}), bf16[128,16,128]{2,0,1:T(8,128)(2,1)S(1)}, u32[]{:S(2)}, u32[]{:S(2)}) async-start(bf16[128,16,128]{2,0,1:T(8,128)(2,1)} %bitcast.135), calls=%async_computation | async-start | bytes 1048576 | tf_op jit(solution)/shard_map/all_to_all | solution.py:63
  153.0 1.0 copy-start.3
  158.1 26.7 %all-to-all-start.2 = ((f32[16,2,2048]{2,1,0:T(2,128)}), f32[16,2,2048]{2,1,0:T(2,128)S(1)}, u32[]{:S(2)}, u32[]{:S(2)}) async-start(f32[16,2,2048]{2,1,0:T(2,128)} %broadcast_in_dim.15), calls=%async_computation.2 | async-start | bytes 524288 | tf_op jit(solution)/shard_map/all_to_all | solution.py:19
  190.7 33.3 %all-to-all-start.3 = ((bf16[16,128,128]{2,1,0:T(8,128)(2,1)}), bf16[16,128,128]{2,1,0:T(8,128)(2,1)S(1)}, u32[]{:S(2)}, u32[]{:S(2)}) async-start(bf16[16,128,128]{2,1,0:T(8,128)(2,1)} %get-tuple-element.36), calls=%async_computation.3 | async-start | bytes 1048576 | tf_op jit(solution)/shard_map/all_to_all | solution.py:61
  201.0 471.5 %all-reduce.2.cloned.1.call-start = ((), (), s32[]{:S(2)}) async-start(), calls=%async_computation.7 | async-start | bytes 1089536 | tf_op jit(solution)/shard_map/psum | solution.py:108
  205.1 583.5 %reduce-scatter.4.cloned.1.call-start = ((), (), s32[]{:S(2)}) async-start(), calls=%async_computation.8 | async-start | bytes 8650752
  242.2 564.2 %copy-start.4 = (f32[16,128,128]{2,1,0:T(8,128)S(1)}, f32[16,128,128]{2,1,0:T(8,128)}, u32[]{:S(2)}) copy-start(f32[16,128,128]{2,1,0:T(8,128)} %get-tuple-element.37) | copy-start | bytes 3145732
  790.7 24.7 %all-to-all-start.4 = ((bf16[16,64,128]{2,1,0:T(8,128)(2,1)}), bf16[16,64,128]{2,1,0:T(8,128)(2,1)S(1)}, u32[]{:S(2)}, u32[]{:S(2)}) async-start(bf16[16,64,128]{2,1,0:T(8,128)(2,1)} %bitcast.29), calls=%async_computation.4 | async-start | bytes 524288 | tf_op jit(solution)/shard_map/all_to_all | solution.py:74
Sparse Core Ops, SparseCore 0:
  40.8 71.3 all-gather.1
  207.2 465.1 all-reduce.1
  677.0 111.4 reduce-scatter.3

commit v2 on v1

v2 whole, which is shorter than its diff:
```python
import functools
import math

import jax
import jax.numpy as jnp
from jax import lax
from jax.experimental import pallas as pl
from jax.experimental.pallas import tpu as pltpu
from jax.sharding import PartitionSpec as P

GW = 2048
GROUPS = 8
BLK = 128
MESH = pl.DeviceIdType.MESH

epsilon = 1e-05
tanh_coef = math.sqrt(2.0 / math.pi)


def sent_to_all(x, axis):
    devices = lax.axis_size(axis)
    return lax.all_to_all(jnp.broadcast_to(x[None], (devices, *x.shape)), axis, 0, 0, tiled=True)


def tail_kernel(
    n_sp, n_dp, stats_ref, mix_ref, dw_ref, stats_out, mix_out, dw_out,
    s_buf, s_own, m_buf, w_buf, b_own, b_buf, c_own,
    s1_send, s1_recv, s2_send, s2_recv, m_send, m_recv, w_send, w_recv,
    b_send, b_recv, c_send, c_recv,
):
    sp = lax.axis_index("sp")
    dp = lax.axis_index("dp")

    def sp_at(d):
        return lax.rem(sp + d, n_sp)

    def dp_at(d):
        return lax.rem(dp + d, n_dp)

    def s1(d):
        return pltpu.make_async_remote_copy(
            stats_ref.at[sp_at(d)], s_buf.at[d], s1_send.at[d], s1_recv.at[d],
            device_id={"sp": sp_at(d)}, device_id_type=MESH)

    def s2(d):
        return pltpu.make_async_remote_copy(
            s_own, stats_out.at[sp], s2_send.at[d], s2_recv.at[d],
            device_id={"sp": sp_at(d)}, device_id_type=MESH)

    def m1(d):
        return pltpu.make_async_remote_copy(
            mix_ref.at[dp_at(d)], m_buf.at[d], m_send.at[d], m_recv.at[d],
            device_id={"dp": dp_at(d)}, device_id_type=MESH)

    def w1(d):
        return pltpu.make_async_remote_copy(
            dw_ref.at[dp_at(d)], w_buf.at[d], w_send.at[d], w_recv.at[d],
            device_id={"dp": dp_at(d)}, device_id_type=MESH)

    def b1(d):
        return pltpu.make_async_remote_copy(
            b_own, b_buf.at[sp], b_send.at[d], b_recv.at[d],
            device_id={"sp": sp_at(d)}, device_id_type=MESH)

    def c1(d):
        return pltpu.make_async_remote_copy(
            c_own, mix_out.at[dp], c_send.at[d], c_recv.at[d],
            device_id={"dp": dp_at(d)}, device_id_type=MESH)

    def each(n, f):
        def step(d, carry):
            f(d)
            return carry

        lax.fori_loop(1, n, step, 0)

    barrier = pltpu.get_barrier_semaphore()
    each(n_sp, lambda d: pl.semaphore_signal(
        barrier, inc=1, device_id={"sp": sp_at(d)}, device_id_type=MESH))
    each(n_dp, lambda d: pl.semaphore_signal(
        barrier, inc=1, device_id={"dp": dp_at(d)}, device_id_type=MESH))
    pl.semaphore_wait(barrier, n_sp + n_dp - 2)

    each(n_sp, lambda d: s1(d).start())
    each(n_dp, lambda d: m1(d).start())
    each(n_dp, lambda d: w1(d).start())

    each(n_sp, lambda d: s1(d).wait_recv())
    s_buf[0] = stats_ref[sp]
    total = jnp.sum(s_buf[...], axis=0)
    s_own[...] = total
    stats_out[sp] = total
    each(n_sp, lambda d: s2(d).start())

    each(n_dp, lambda d: m1(d).wait_recv())
    m_buf[0] = mix_ref[dp]
    plane = jnp.sum(m_buf[...], axis=0)
    b_own[...] = plane
    b_buf[sp] = plane
    each(n_sp, lambda d: b1(d).start())

    each(n_dp, lambda d: w1(d).wait_recv())
    w_buf[0] = dw_ref[dp]
    dw_out[...] = jnp.sum(w_buf[...].astype(jnp.float32), axis=0)

    each(n_sp, lambda d: b1(d).wait_recv())
    per = n_sp // GROUPS
    joined = jnp.sum(b_buf[...].reshape(GROUPS, per, 8, BLK), axis=1)
    rows = lax.broadcasted_iota(jnp.int32, (GROUPS, 8, BLK), 1)
    own_plane = jnp.broadcast_to(b_own[...][None], (GROUPS, 8, BLK))
    sent = jnp.where(rows >= 5, own_plane, joined).reshape(GROUPS * 8, BLK).astype(jnp.bfloat16)
    c_own[...] = sent
    mix_out[dp] = sent
    each(n_dp, lambda d: c1(d).start())

    each(n_sp, lambda d: s2(d).wait_recv())
    each(n_dp, lambda d: c1(d).wait_recv())
    each(n_sp, lambda d: s1(d).wait_send())
    each(n_sp, lambda d: s2(d).wait_send())
    each(n_sp, lambda d: b1(d).wait_send())
    each(n_dp, lambda d: m1(d).wait_send())
    each(n_dp, lambda d: w1(d).wait_send())
    each(n_dp, lambda d: c1(d).wait_send())


def finish(stats, mix, dw):
    n_sp, n_dp = lax.axis_size("sp"), lax.axis_size("dp")
    vmem = pl.BlockSpec(memory_space=pltpu.VMEM)
    f32 = jnp.float32
    dma = pltpu.SemaphoreType.DMA
    return pl.pallas_call(
        functools.partial(tail_kernel, n_sp, n_dp),
        out_shape=(
            jax.ShapeDtypeStruct(stats.shape, f32),
            jax.ShapeDtypeStruct((n_dp, GROUPS * 8, BLK), jnp.bfloat16),
            jax.ShapeDtypeStruct(dw.shape[1:], f32),
        ),
        in_specs=[vmem] * 3,
        out_specs=(vmem,) * 3,
        scratch_shapes=[
            pltpu.VMEM(stats.shape, f32),
            pltpu.VMEM(stats.shape[1:], f32),
            pltpu.VMEM(mix.shape, f32),
            pltpu.VMEM(dw.shape, jnp.bfloat16),
            pltpu.VMEM(mix.shape[1:], f32),
            pltpu.VMEM((n_sp, *mix.shape[1:]), f32),
            pltpu.VMEM((GROUPS * 8, BLK), jnp.bfloat16),
            dma((n_sp,)), dma((n_sp,)), dma((n_sp,)), dma((n_sp,)),
            dma((n_dp,)), dma((n_dp,)), dma((n_dp,)), dma((n_dp,)),
            dma((n_sp,)), dma((n_sp,)), dma((n_dp,)), dma((n_dp,)),
        ],
        compiler_params=pltpu.CompilerParams(collective_id=1, has_side_effects=True),
    )(stats, mix, dw)


def gelu_slope(values):
    inner = tanh_coef * (values + 0.044715 * values * values * values)
    hyper = jnp.tanh(inner)
    return 0.5 * (1.0 + hyper) + 0.5 * values * (1.0 - hyper * hyper) * tanh_coef * (
        1.0 + 3.0 * 0.044715 * values * values
    )


def local(cotangent, unit_pre, gate_pre, out_weight, mix_weight, mix_bias, norm_gain, norm_shift):
    seq_len = unit_pre.shape[1]
    channels = unit_pre.shape[2]
    group_dim = GW // GROUPS
    blocks = seq_len // BLK
    n_dp = lax.axis_size("dp")
    group = lax.axis_index("sp") * channels // group_dim
    units = unit_pre[0].astype(jnp.float32)
    gates = gate_pre[0].astype(jnp.float32)
    unit_act = jax.nn.gelu(units)
    gate_act = jax.nn.gelu(gates)
    moments = sent_to_all(
        jnp.stack([jnp.sum(gate_act, axis=-1), jnp.sum(gate_act * gate_act, axis=-1)]), "sp"
    ).sum(axis=0)
    mean_val = moments[0] / GW
    var_val = moments[1] / GW - mean_val * mean_val
    rstd_val = lax.rsqrt(var_val + epsilon)
    centred = (gate_act - mean_val[:, None]) * rstd_val[:, None]
    gain_vec = norm_gain.astype(jnp.float32)
    normed = (centred * gain_vec + norm_shift.astype(jnp.float32)).astype(jnp.bfloat16)
    causal = jnp.arange(BLK)[:, None] >= jnp.arange(BLK)[None, :]
    local_weight = lax.dynamic_index_in_dim(mix_weight, group, 0, keepdims=False)
    masked = jnp.where(causal, local_weight, jnp.zeros_like(local_weight))
    local_bias = lax.dynamic_index_in_dim(mix_bias, group, 0, keepdims=False).astype(jnp.float32)
    normed_blocks = normed.reshape(blocks, BLK, channels)
    mixed = jnp.einsum("ts,nsd->ntd", masked, normed_blocks, preferred_element_type=jnp.float32)
    mixed = (mixed + local_bias[None, :, None]).reshape(seq_len, channels)
    gated = (unit_act * mixed).astype(jnp.bfloat16)
    weight_whole = sent_to_all(out_weight, "dp").reshape(-1, channels)
    dy_rows = lax.all_gather(cotangent, "sp", axis=1, tiled=True)[0]
    head = jnp.dot(dy_rows, weight_whole, preferred_element_type=jnp.float32)
    weight_part = lax.dot_general(
        dy_rows, gated, (((0,), (0,)), ((), ())), preferred_element_type=jnp.float32
    ).astype(jnp.bfloat16)
    token_count = n_dp * seq_len
    norm_scale = 1.0 / math.sqrt(token_count)
    mix_scale = 1.0 / math.sqrt(token_count // BLK * group_dim)
    unit_grad = (head * mixed * gelu_slope(units)).astype(jnp.bfloat16)
    mix_grad = head * unit_act
    mix_round = mix_grad.astype(jnp.bfloat16).reshape(blocks, BLK, channels)
    mix_term = jnp.einsum("ntd,nsd->ts", mix_round, normed_blocks, preferred_element_type=jnp.float32)
    mix_term = jnp.where(causal, mix_term, jnp.float32(0.0))
    bias_term = jnp.sum(mix_grad.reshape(blocks, BLK, channels), axis=(0, 2))
    normed_grad = jnp.einsum(
        "ts,ntd->nsd", masked, mix_round, preferred_element_type=jnp.float32
    ).reshape(seq_len, channels)
    gain_term = jnp.sum(normed_grad * centred, axis=0)
    shift_term = jnp.sum(normed_grad, axis=0)
    scaled = normed_grad * gain_vec
    stats = jnp.stack(
        [
            jnp.sum(scaled, axis=-1).reshape(blocks, BLK),
            jnp.sum(scaled * centred, axis=-1).reshape(blocks, BLK),
        ],
        axis=1,
    )
    small = jnp.stack([bias_term, gain_term, shift_term, jnp.zeros_like(bias_term)])
    first = (jnp.arange(n_dp) == 0)[:, None, None]
    packed = jnp.concatenate(
        [mix_term.reshape(n_dp, BLK // n_dp, BLK), jnp.where(first, small[None], 0.0)], axis=1
    )
    back_sums, mix_all, dw_sum = finish(stats, packed, weight_part.reshape(n_dp, -1, channels))
    first_m = back_sums[:, 0].reshape(seq_len) / GW
    second_m = back_sums[:, 1].reshape(seq_len) / GW
    gate_grad = (
        rstd_val[:, None]
        * (scaled - first_m[:, None] - centred * second_m[:, None])
        * gelu_slope(gates)
    ).astype(jnp.bfloat16)
    mix_all = mix_all.reshape(n_dp, GROUPS, 8, BLK).astype(jnp.float32)
    lines = BLK // n_dp
    weight_total = jnp.swapaxes(mix_all[:, :, :lines], 0, 1).reshape(GROUPS, BLK, BLK)
    return (
        unit_grad[None],
        gate_grad[None],
        dw_sum * norm_scale,
        weight_total * mix_scale,
        mix_all[0, :, 4] * mix_scale,
        mix_all[0, 0, 5] * norm_scale,
        mix_all[0, 0, 6] * norm_scale,
    )


def solution(mesh):
    return jax.shard_map(
        local,
        mesh=mesh,
        in_specs=(
            P("dp", "sp", None),
            P("dp", None, "sp"),
            P("dp", None, "sp"),
            P("dp", "sp"),
            P(),
            P(),
            P("sp"),
            P("sp"),
        ),
        out_specs=(P("dp", None, "sp"), P("dp", None, "sp"), P("dp", "sp"), P(), P(), P("sp"), P("sp")),
        check_vma=False,
    )
```

time: 830 us -> 196 us (0.24)
  waiting for transfers between devices: 670 us -> 78.5 us
  Pallas kernels: 0 us -> 38.4 us
  blocking collectives: 33.5 us -> 0 us
  starting transfers between devices: 53.6 us -> 30 us
  local copies, waits for them, and re-layouts: 19.8 us -> 4.42 us
    psum x1 -> x0, waiting for transfers between devices: 430 us -> none  [local(): total = lax.psum(packed, ('sp', 'dp'))]
    unnamed x4 -> x1, waiting for transfers between devices: 115 us -> 0.68 us
    all_to_all x5 -> x2, waiting for transfers between devices: 62 us -> 18.6 us  [sent_to_all(): lax.all_to_all(jnp.broadcast_to(x[None], (devices, *x.shape)), axis, 0, 0...]
    pallas_call x0 -> x1, Pallas kernels: none -> 38.4 us  [finish(): pl.pallas_call(functools.partial(tail_kernel, n_sp, n_dp), out_shape=(jax...]
    all_gather x1 -> x0, blocking collectives: 33.5 us -> none  [local(): weight_rows = lax.all_gather(out_weight, 'sp', axis=1, tiled=True)]
    all_to_all x5 -> x2, starting transfers between devices: 53.5 us -> 30 us  [sent_to_all(): lax.all_to_all(jnp.broadcast_to(x[None], (devices, *x.shape)), axis, 0, 0...]
    unnamed x18 -> x6, local copies, waits for them, and re-layouts: 15.4 us -> 0.02 us
  transfers between devices with their start and end apart: 8 -> 3, of which waited for: 7 -> 3; matrix products, arithmetic and copies ran while one was open for 5% -> 6% of each run, Pallas kernels for 0% -> 0%
where the time goes in v2:
time: 196 us; the launch traced here: 195 us
  waiting for transfers between devices  78.5 us (40%)
  Pallas kernels  38.4 us (20%)
  starting transfers between devices  30 us (15%)
  matrix products  14.7 us (8%)
  other arithmetic  14.6 us (7%)
  between operations  14.2 us (7%)
  local copies, waits for them, and re-layouts  4.42 us (2%)
    all_gather x1, waiting for transfers between devices, local(): dy_rows = lax.all_gather(cotangent, 'sp', axis=1, tiled=True)[0]  59.2 us
    pallas_call x1, Pallas kernels, finish(): pl.pallas_call(functools.partial(tail_kernel, n_sp, n_dp), out_shape=(jax...  38.4 us
    all_to_all x2, starting transfers between devices, sent_to_all(): lax.all_to_all(jnp.broadcast_to(x[None], (devices, *x.shape)), axis, 0, 0...  30 us
    all_to_all x2, waiting for transfers between devices, sent_to_all(): lax.all_to_all(jnp.broadcast_to(x[None], (devices, *x.shape)), axis, 0, 0...  18.6 us
    dot_general x1, matrix products, local(): head = jnp.dot(dy_rows, weight_whole, preferred_element_type=jnp.float32)  7.69 us
  transfers between devices with their start and end apart: 3, of which 3 were waited for; matrix products, arithmetic and copies ran while one was open for 6% of the time, Pallas kernels for 0%

profile of v2, /device:TPU:1, one launch (start us, length us, event | category | flops | bytes accessed | tf_op | source)
XLA Modules:
  0.0 194.9 jit_solution(1793807013383277503)
XLA Ops:
  7.2 0.7 all-gather.2.cloned.1.call-update
  7.9 1.8 fusion.76
  9.7 0.8 broadcast_in_dim.26
  10.5 15.7 %all-to-all-start.1 = ((f32[16,2,2048]{2,1,0:T(2,128)}), f32[16,2,2048]{2,1,0:T(2,128)S(1)}, u32[]{:S(2)}, u32[]{:S(2)}) async-start(f32[16,2,2048]{2,1,0:T(2,128)} %broadcast_in_dim.26), calls=%async_computation.1 | async-start | bytes 524288 | tf_op jit(solution)/shard_map/all_to_all | solution.py:22
  26.3 0.7 convert_element_type.94
  26.9 0.7 convert_element_type.95
  27.7 0.7 bitcast_convert_fusion.1
  28.4 11.7 %all-to-all-done.1 = f32[16,2,2048]{2,1,0:T(2,128)S(1)} async-done(((f32[16,2,2048]{2,1,0:T(2,128)}), f32[16,2,2048]{2,1,0:T(2,128)S(1)}, u32[]{:S(2)}, u32[]{:S(2)}) %all-to-all-start.1) | async-done | bytes 262176 | tf_op jit(solution)/shard_map/all_to_all | solution.py:22
  40.0 1.6 broadcast_in_dim.25
  41.7 14.3 %all-to-all-start = ((bf16[32,64,128]{2,1,0:T(8,128)(2,1)}), bf16[32,64,128]{2,1,0:T(8,128)(2,1)S(1)}, u32[]{:S(2)}, u32[]{:S(2)}) async-start(bf16[32,64,128]{2,1,0:T(8,128)(2,1)} %broadcast_in_dim.25), calls=%async_computation | async-start | bytes 1048576 | tf_op jit(solution)/shard_map/all_to_all | solution.py:22
  56.1 1.7 add_convert_fusion.1
  57.8 2.7 %fusion.47 = (bf16[16,128,128]{2,1,0:T(8,128)(2,1)S(1)}, f32[16,128,128]{1,2,0:T(8,128)}) fusion(f32[128]{0:T(128)S(1)} %bitcast_convert_fusion.1, bf16[16,128,128]{2,1,0:T(8,128)(2,1)S(1)} %bitcast.153, bf16[8,128,128]{2,1,0:T(8,128)(2,1)} %param.12, s32[]{:T(128)S(6)} %select_n.28, bf16[16,128,128]{2,1,0:T(8,128)(2,1)} %bitcast.175), kind=kOutput, calls=%fused_computation.62 | convolution fusion | flops 70287360 | bytes 2654724 | tf_op jit(solution)/shard_map/ts,nsd->ntd/dot_general | solution.py:189
  60.4 6.9 %all-to-all-done = bf16[32,64,128]{2,1,0:T(8,128)(2,1)S(1)} async-done(((bf16[32,64,128]{2,1,0:T(8,128)(2,1)}), bf16[32,64,128]{2,1,0:T(8,128)(2,1)S(1)}, u32[]{:S(2)}, u32[]{:S(2)}) %all-to-all-start) | async-done | bytes 524320 | tf_op jit(solution)/shard_map/all_to_all | solution.py:22
  67.4 59.2 %all-gather.2.cloned.1.call-done = bf16[1,2048,2048]{2,1,0:T(8,128)(2,1)} async-done(((bf16[1,128,2048]{2,1,0:T(8,128)(2,1)}), bf16[1,2048,2048]{2,1,0:T(8,128)(2,1)}) %all-gather.2.cloned.1.call-update) | async-done | bytes 8388624 | tf_op jit(solution)/shard_map/all_gather | solution.py:193
  126.6 7.7 %fusion.80 = (f32[2048]{0:T(1024)S(1)}, bf16[2048,128]{1,0:T(8,128)(2,1)S(1)}, bf16[2048,128]{1,0:T(8,128)(2,1)}) fusion(bf16[1,2048,128]{2,1,0:T(8,128)(2,1)S(1)} %copy-done.2, f32[16,128,128]{1,2,0:T(8,128)} %get-tuple-element.30, bf16[2048,128]{1,0:T(8,128)(2,1)S(1)} %bitcast.154, bf16[1,2048,2048]{2,1,0:T(8,128)(2,1)} %all-gather.2.cloned.1.call-done), kind=kOutput, calls=%fused_computation.106 | convolution fusion | flops 1082128384 | bytes 11542528 | tf_op jit(solution)/shard_map/dot_general | solution.py:194
  134.3 1.3 fusion.7
  135.6 1.0 copy.25
  136.6 2.2 %fusion.72 = (f32[128]{0:T(128)S(1)}, f32[16,128]{1,0:T(8,128)S(1)}, f32[16,128]{1,0:T(8,128)S(1)}, f32[16,128,128]{2,1,0:T(8,128)S(1)}, f32[16,128,128]{1,2,0:T(8,128)S(1)}) fusion(f32[16,128]{1,0:T(8,128)S(1)} %add_rsqrt_fusion, f32[16,128]{1,0:T(8,128)S(1)} %bitcast.159, f32[128]{0:T(128)S(1)} %convert_element_type.94, ...), kind=kOutput, calls=%fused_computation.91 | convolution fusion | flops 71593856 | bytes 3212292 | tf_op jit(solution)/shard_map/ts,ntd->nsd/dot_general | solution.py:207
  138.8 0.8 fusion.14
  139.6 0.3 reduce_sum.88
  139.9 0.6 pad_maximum_fusion.2.stats_ref
  140.6 0.1 broadcast_select_fusion
  140.7 0.7 pad_maximum_fusion.mix_ref
  141.4 38.4 %shard_map.135 = (f32[16,2,128]{2,1,0:T(2,128)}, bf16[32,64,128]{2,1,0:T(8,128)(2,1)}, f32[64,128]{1,0:T(8,128)}) custom-call(f32[16,2,128]{2,1,0:T(2,128)} %pad_maximum_fusion.2.stats_ref, f32[32,8,128]{2,1,0:T(8,128)} %pad_maximum_fusion.mix_ref, bf16[32,64,128]{2,1,0:T(8,128)(2,1)} %bitcast.151), custom_call_target="tpu_custom_call" | custom-call | tf_op jit(solution)/shard_map/pallas_call | solution.py:131
  179.9 1.1 bitcast_convert_fusion
  181.0 0.5 fusion.89
  181.6 0.1 fusion.77
  181.7 0.8 slice_multiply_fusion.4
  182.5 1.4 broadcast_multiply_fusion
  183.9 0.9 copy.26
  184.8 0.6 multiply_bitcast_fusion
  185.4 2.7 %fusion.67 = bf16[1,2048,128]{2,1,0:T(8,128)(2,1)} fusion(bf16[1,2048,128]{2,1,0:T(8,128)(2,1)S(1)} %copy-done.1, f32[16,128,128]{1,2,0:T(8,128)S(1)} %get-tuple-element.28, f32[2048]{0:T(1024)S(1)} %bitcast.166, f32[2048]{0:T(1024)S(1)} %bitcast.165, f32[128]{0:T(128)S(1)} %convert_element_type.94, f32[2048]{0:T(1024)S(1)} %add_rsqrt_fusion.1, ...), kind=kLoop, calls=%fused_computation.82 | loop fusion | flops 9175040 | bytes 2130432 | tf_op jit(solution)/shard_map/convert_element_type | solution.py:232
  (17 shorter events, 0.4 us)
Async XLA Ops:
  7.2 119.4 %copy-start.2 = (bf16[1,2048,128]{2,1,0:T(8,128)(2,1)S(1)}, bf16[1,2048,128]{2,1,0:T(8,128)(2,1)}, u32[]{:S(2)}) copy-start(bf16[1,2048,128]{2,1,0:T(8,128)(2,1)} %param.9) | copy-start | bytes 1572868
  7.2 119.4 %all-gather.2.cloned.1.call-start = ((), (), s32[]{:S(2)}) async-start(), calls=%async_computation.2 | async-start | bytes 8912896 | tf_op jit(solution)/shard_map/all_gather | solution.py:193
  10.5 29.5 %all-to-all-start.1 = ((f32[16,2,2048]{2,1,0:T(2,128)}), f32[16,2,2048]{2,1,0:T(2,128)S(1)}, u32[]{:S(2)}, u32[]{:S(2)}) async-start(f32[16,2,2048]{2,1,0:T(2,128)} %broadcast_in_dim.26), calls=%async_computation.1 | async-start | bytes 524288 | tf_op jit(solution)/shard_map/all_to_all | solution.py:22
  41.7 25.7 %all-to-all-start = ((bf16[32,64,128]{2,1,0:T(8,128)(2,1)}), bf16[32,64,128]{2,1,0:T(8,128)(2,1)S(1)}, u32[]{:S(2)}, u32[]{:S(2)}) async-start(bf16[32,64,128]{2,1,0:T(8,128)(2,1)} %broadcast_in_dim.25), calls=%async_computation | async-start | bytes 1048576 | tf_op jit(solution)/shard_map/all_to_all | solution.py:22
  126.6 7.7 %copy-start = (bf16[1,2048,2048]{2,1,0:T(8,128)(2,1)S(1)}, bf16[1,2048,2048]{2,1,0:T(8,128)(2,1)}, u32[]{:S(2)}) copy-start(bf16[1,2048,2048]{2,1,0:T(8,128)(2,1)} %all-gather.2.cloned.1.call-done) | copy-start | bytes 25165828
  134.3 2.3 %copy-start.1 = (bf16[1,2048,128]{2,1,0:T(8,128)(2,1)S(1)}, bf16[1,2048,128]{2,1,0:T(8,128)(2,1)}, u32[]{:S(2)}) copy-start(bf16[1,2048,128]{2,1,0:T(8,128)(2,1)} %param.10) | copy-start | bytes 1572868
Sparse Core Ops, SparseCore 0:
  10.1 116.4 all-gather.1

commit v3 on v1

v3 whole, which is shorter than its diff:
```python
import functools
import math

import jax
import jax.numpy as jnp
from jax import lax
from jax.experimental import pallas as pl
from jax.experimental.pallas import tpu as pltpu
from jax.sharding import PartitionSpec as P

GROUPS = 8
BLK = 128
MESH = pl.DeviceIdType.MESH
F32 = jnp.float32
BF16 = jnp.bfloat16

epsilon = 1e-05
tanh_coef = math.sqrt(2.0 / math.pi)
SLABS = BLK // 8


def gelu_pair(x):
    hyper = jnp.tanh(tanh_coef * (x + 0.044715 * x * x * x))
    value = 0.5 * x * (1.0 + hyper)
    slope = 0.5 * (1.0 + hyper) + 0.5 * x * (1.0 - hyper * hyper) * tanh_coef * (
        1.0 + 3.0 * 0.044715 * x * x
    )
    return value, slope


def dot(a, b, ca, cb, precision=None):
    return lax.dot_general(
        a, b, (((ca,), (cb,)), ((), ())), preferred_element_type=F32, precision=precision
    )


def row_sums(a, b):
    rows = lax.broadcasted_iota(jnp.int32, (8, 2 * BLK), 0)
    lanes = lax.broadcasted_iota(jnp.int32, (8, 2 * BLK), 1)
    pick = jnp.where(rows == lanes // BLK, 1.0, 0.0).astype(F32)
    both = jnp.concatenate([a, b], axis=1)
    return dot(pick, both, 1, 1, lax.Precision.HIGHEST)[0:2]


def as_columns(pair):
    rows = lax.broadcasted_iota(jnp.int32, (8, 2 * BLK), 0)
    lanes = lax.broadcasted_iota(jnp.int32, (8, 2 * BLK), 1)
    pick = jnp.where(rows == lanes // BLK, 1.0, 0.0).astype(F32)
    padded = jnp.concatenate([pair, jnp.zeros((6, BLK), F32)], axis=0)
    wide = dot(padded, pick, 0, 0, lax.Precision.HIGHEST)
    return wide[:, :BLK], wide[:, BLK:]


def kernel(
    n_sp, n_dp, units_all, norm_scale, mix_scale,
    cot_ref, unit_ref, gate_ref, w_ref, mixw_ref, mixb_ref, gain_ref, shift_ref,
    ugrad_ref, ggrad_ref, dw_out, mix_out, bias_out, gain_out, shift_out,
    gbuf, w_all, gact_s, st_src, st_buf, st_own, st_all,
    bs_src, bs_buf, bs_own, bs_all, masked_s, masked_t, bias_s,
    dwt, scaled_s, cent_s, rs_s, mixacc, bacc, gacc, sacc,
    mix_src, m_buf, w_src, w_buf, b_own, b_buf, c_own, c_buf,
    r_send, r_recv, l_send, l_recv, wa_send, wa_recv,
    f1_send, f1_recv, f2_send, f2_recv, s1_send, s1_recv, s2_send, s2_recv,
    m_send, m_recv, w_send, w_recv, b_send, b_recv, c_send, c_recv,
):
    sp = lax.axis_index("sp")
    dp = lax.axis_index("dp")
    depth = cot_ref.shape[2]
    last = 2 * (n_sp // 2 - 1)

    def sp_at(d):
        return lax.rem(sp + d, n_sp)

    def dp_at(d):
        return lax.rem(dp + d, n_dp)

    right, left = sp_at(1), sp_at(n_sp - 1)

    def each(n, f):
        def step(d, carry):
            f(d)
            return carry

        lax.fori_loop(1, n, step, 0)

    def over_sp(src, dst, send, recv, d):
        return pltpu.make_async_remote_copy(
            src, dst, send.at[d], recv.at[d], device_id={"sp": sp_at(d)}, device_id_type=MESH)

    def over_dp(src, dst, send, recv, d):
        return pltpu.make_async_remote_copy(
            src, dst, send.at[d], recv.at[d], device_id={"dp": dp_at(d)}, device_id_type=MESH)

    def f1(d):
        return over_sp(st_src.at[sp_at(d)], st_buf.at[d], f1_send, f1_recv, d)

    def f2(d):
        return over_sp(st_own, st_all.at[sp], f2_send, f2_recv, d)

    def s1(d):
        return over_sp(bs_src.at[sp_at(d)], bs_buf.at[d], s1_send, s1_recv, d)

    def s2(d):
        return over_sp(bs_own, bs_all.at[sp], s2_send, s2_recv, d)

    def wa(d):
        return over_dp(w_ref, w_all.at[dp], wa_send, wa_recv, d)

    def m1(d):
        return over_dp(mix_src.at[dp_at(d)], m_buf.at[d], m_send, m_recv, d)

    def w1(d):
        return over_dp(w_src.at[dp_at(d)], w_buf.at[d], w_send, w_recv, d)

    def b1(d):
        return over_sp(b_own, b_buf.at[sp], b_send, b_recv, d)

    def c1(d):
        return over_dp(c_own, c_buf.at[dp], c_send, c_recv, d)

    def to_right(src, at, c):
        return pltpu.make_async_remote_copy(
            src, gbuf.at[at], r_send.at[c], r_recv.at[c],
            device_id={"sp": right}, device_id_type=MESH)

    def to_left(src, at, c):
        return pltpu.make_async_remote_copy(
            src, gbuf.at[at], l_send.at[c], l_recv.at[c],
            device_id={"sp": left}, device_id_type=MESH)

    def came_right(c):
        at = 2 * sp_at(n_sp - 1 - c // 2) + lax.rem(c, 2)
        return at, to_right(gbuf.at[at], at, c)

    def came_left(c):
        at = 2 * sp_at(1 + c // 2) + 1 - lax.rem(c, 2)
        return at, to_left(gbuf.at[at], at, c)

    barrier = pltpu.get_barrier_semaphore()
    each(n_sp, lambda d: pl.semaphore_signal(
        barrier, inc=1, device_id={"sp": sp_at(d)}, device_id_type=MESH))
    each(n_dp, lambda d: pl.semaphore_signal(
        barrier, inc=1, device_id={"dp": dp_at(d)}, device_id_type=MESH))

    def gate_sums(p, carry):
        rows = pl.ds(pl.multiple_of(p * BLK, BLK), BLK)
        act, _ = gelu_pair(gate_ref[rows, :].astype(F32))
        gact_s[rows, :] = act
        st_src[p] = row_sums(act, act * act)
        return carry

    lax.fori_loop(0, n_sp, gate_sums, 0)
    pl.semaphore_wait(barrier, n_sp + n_dp - 2)

    each(n_sp, lambda d: f1(d).start())
    for c in range(2):
        to_right(cot_ref.at[c], 2 * sp + c, c).start()
        to_left(cot_ref.at[1 - c], 2 * sp + 1 - c, c).start()
    each(n_dp, lambda d: wa(d).start())

    for c in range(2):
        gbuf[2 * sp + c] = cot_ref[c]
    w_all[dp] = w_ref[...]
    group = sp * GROUPS // n_sp
    t_at = lax.broadcasted_iota(jnp.int32, (BLK, BLK), 0)
    s_at = lax.broadcasted_iota(jnp.int32, (BLK, BLK), 1)
    causal = t_at >= s_at
    masked = jnp.where(causal, mixw_ref[group].astype(F32), 0.0)
    masked_s[...] = masked.astype(BF16)
    masked_t[...] = jnp.transpose(masked).astype(BF16)
    picked = lax.broadcasted_iota(jnp.int32, (GROUPS, BLK), 0) == group
    bias_row = jnp.where(picked, mixb_ref[...].astype(F32), 0.0)
    bias_s[...] = dot(bias_row, jnp.ones((GROUPS, BLK), F32), 0, 0, lax.Precision.HIGHEST)
    for acc in (mixacc, bacc, gacc, sacc, dwt, mix_src):
        acc[...] = jnp.zeros_like(acc)

    each(n_sp, lambda d: f1(d).wait_recv())
    st_buf[0] = st_src[sp]
    moments = jnp.sum(st_buf[...], axis=0) * (1.0 / units_all)
    mean_row = moments[0:1]
    rstd_row = lax.rsqrt(moments[1:2] - mean_row * mean_row + epsilon)
    norm_row = jnp.concatenate([mean_row, rstd_row], axis=0)
    st_own[...] = norm_row
    st_all[sp] = norm_row
    each(n_sp, lambda d: f2(d).start())

    def block(b, carry):
        far = (b + 1) // 2
        d = jnp.where(lax.rem(b, 2) == 1, n_sp - far, far)
        p = sp_at(d)
        rows = pl.ds(pl.multiple_of(p * BLK, BLK), BLK)
        gain = gain_ref[...].astype(F32)
        unit_act, unit_slope = gelu_pair(unit_ref[rows, :].astype(F32))
        _, gate_slope = gelu_pair(gate_ref[rows, :].astype(F32))
        mean, rstd = as_columns(st_all[p])
        centred = (gact_s[rows, :] - mean) * rstd
        normed = (centred * gain + shift_ref[...].astype(F32)).astype(BF16)
        mixed = dot(masked_s[...], normed, 1, 0) + bias_s[...]
        gated = (unit_act * mixed).astype(BF16)
        dy = gbuf[pl.ds(2 * p, 2)].reshape(BLK, depth)
        head = dot(dy, w_all[...].reshape(depth, BLK), 1, 0)
        dwt[...] += dot(gated, dy, 0, 0)
        ugrad_ref[rows, :] = (head * mixed * unit_slope).astype(BF16)
        mix_grad = head * unit_act
        mix_round = mix_grad.astype(BF16)
        mixacc[...] += dot(mix_round, normed, 1, 1)
        bacc[...] += mix_grad
        normed_grad = dot(masked_t[...], mix_round, 1, 0)
        gacc[...] += normed_grad * centred
        sacc[...] += normed_grad
        scaled = normed_grad * gain
        scaled_s[rows, :] = scaled
        cent_s[rows, :] = centred
        rs_s[rows, :] = rstd * gate_slope
        bs_src[p] = row_sums(scaled, scaled * centred)

        @pl.when(b > 0)
        def _():
            s1(d).start()

        return carry

    def step(q, carry):
        @pl.when(q < last)
        def _():
            at, came = came_right(q)
            came.wait_recv()

            @pl.when(q < last - 1)
            def _():
                to_right(gbuf.at[at], at, q + 2).start()

            at_left, came_l = came_left(q)
            came_l.wait_recv()

            @pl.when(q < last - 1)
            def _():
                to_left(gbuf.at[at_left], at_left, q + 2).start()

        @pl.when(q == 2)
        def _():
            each(n_sp, lambda d: f2(d).wait_recv())
            each(n_dp, lambda d: wa(d).wait_recv())

        @pl.when(q == last + 1)
        def _():
            came_right(last)[1].wait_recv()
            came_left(last)[1].wait_recv()

        lo = jnp.maximum(0, jnp.minimum(2 * (q - 2), q))
        hi = jnp.maximum(0, jnp.minimum(2 * (q - 2) + 2, q + 1))
        lax.fori_loop(lo, hi, block, 0)
        return carry

    lax.fori_loop(0, n_sp, step, 0)

    mix_src[0:SLABS] = jnp.where(causal, mixacc[...], 0.0).reshape(SLABS, 8, BLK)
    bias_sum = dot(jnp.ones((8, BLK), F32), bacc[...], 1, 1, lax.Precision.HIGHEST)[0:1]
    mix_src[SLABS] = jnp.concatenate(
        [
            bias_sum,
            jnp.sum(gacc[...], axis=0, keepdims=True),
            jnp.sum(sacc[...], axis=0, keepdims=True),
            jnp.zeros((5, BLK), F32),
        ],
        axis=0,
    )
    each(n_dp, lambda d: m1(d).start())

    piece = depth // n_dp
    per_tile = BLK // piece

    for j in range(depth // BLK):
        tile = jnp.transpose(dwt[:, j * BLK : (j + 1) * BLK]).astype(BF16)
        w_src[j * per_tile : (j + 1) * per_tile] = tile.reshape(per_tile, piece, BLK)
    each(n_dp, lambda d: w1(d).start())

    each(n_sp, lambda d: s1(d).wait_recv())
    bs_buf[0] = bs_src[sp]
    back = jnp.sum(bs_buf[...], axis=0) * (1.0 / units_all)
    bs_own[...] = back
    bs_all[sp] = back
    each(n_sp, lambda d: s2(d).start())

    each(n_dp, lambda d: m1(d).wait_recv())
    m_buf[0] = mix_src[dp]
    plane = jnp.sum(m_buf[...], axis=0)
    b_own[...] = plane
    b_buf[sp] = plane

    @pl.when(dp <= SLABS)
    def _():
        each(n_sp, lambda d: b1(d).start())

    each(n_dp, lambda d: w1(d).wait_recv())
    w_buf[0] = w_src[dp]
    dw_out[...] = jnp.sum(w_buf[...].astype(F32), axis=0) * norm_scale

    @pl.when(dp <= SLABS)
    def _():
        each(n_sp, lambda d: b1(d).wait_recv())
        joined = jnp.sum(b_buf[...].reshape(GROUPS, n_sp // GROUPS, 8, BLK), axis=1)
        at = lax.broadcasted_iota(jnp.int32, (GROUPS, 8, BLK), 1)
        own = jnp.broadcast_to(b_own[...][None], (GROUPS, 8, BLK))
        keep = jnp.logical_and(at >= 1, dp == SLABS)
        sent = jnp.where(keep, own, joined).reshape(GROUPS * 8, BLK).astype(BF16)
        c_own[...] = sent
        c_buf[dp] = sent
        each(n_dp, lambda d: c1(d).start())

    each(n_sp, lambda d: s2(d).wait_recv())

    def gate_block(p, carry):
        rows = pl.ds(pl.multiple_of(p * BLK, BLK), BLK)
        first_m, second_m = as_columns(bs_all[p])
        inner = scaled_s[rows, :] - first_m - cent_s[rows, :] * second_m
        ggrad_ref[rows, :] = (inner * rs_s[rows, :]).astype(BF16)
        return carry

    lax.fori_loop(0, n_sp, gate_block, 0)

    def c_came(d):
        @pl.when(dp_at(n_dp - d) <= SLABS)
        def _():
            c1(d).wait_recv()

    each(n_dp, c_came)
    for i in range(SLABS):
        mix_out[:, 8 * i : 8 * i + 8, :] = (
            c_buf[i].astype(F32).reshape(GROUPS, 8, BLK) * mix_scale
        )
    small = c_buf[SLABS].astype(F32)
    bias_out[...] = jnp.concatenate(
        [small[8 * g : 8 * g + 1] for g in range(GROUPS)], axis=0
    ) * mix_scale
    gain_out[...] = small[1:2] * norm_scale
    shift_out[...] = small[2:3] * norm_scale

    for c in range(2):
        to_right(cot_ref.at[c], 2 * sp + c, c).wait_send()
        to_left(cot_ref.at[1 - c], 2 * sp + 1 - c, c).wait_send()

    def ring_sent(c, carry):
        at = came_right(c - 2)[0]
        to_right(gbuf.at[at], at, c).wait_send()
        at = came_left(c - 2)[0]
        to_left(gbuf.at[at], at, c).wait_send()
        return carry

    lax.fori_loop(2, last + 1, ring_sent, 0)
    each(n_sp, lambda d: f1(d).wait_send())
    each(n_sp, lambda d: f2(d).wait_send())
    each(n_sp, lambda d: s1(d).wait_send())
    each(n_sp, lambda d: s2(d).wait_send())
    each(n_dp, lambda d: wa(d).wait_send())
    each(n_dp, lambda d: m1(d).wait_send())
    each(n_dp, lambda d: w1(d).wait_send())

    @pl.when(dp <= SLABS)
    def _():
        each(n_sp, lambda d: b1(d).wait_send())
        each(n_dp, lambda d: c1(d).wait_send())


def local(cotangent, unit_pre, gate_pre, out_weight, mix_weight, mix_bias, norm_gain, norm_shift):
    n_sp, n_dp = lax.axis_size("sp"), lax.axis_size("dp")
    seq_len, channels = unit_pre.shape[1:]
    depth = cotangent.shape[2]
    units_all = channels * n_sp
    token_count = n_dp * seq_len
    norm_scale = 1.0 / math.sqrt(token_count)
    mix_scale = 1.0 / math.sqrt(token_count // BLK * (units_all // GROUPS))
    piece = depth // n_dp
    vmem = pl.BlockSpec(memory_space=pltpu.VMEM)
    dma = pltpu.SemaphoreType.DMA
    tile = (BLK, BLK)
    chunks = n_sp - 1

    def shape(dims, dtype=F32):
        return jax.ShapeDtypeStruct(dims, dtype)

    outs = pl.pallas_call(
        functools.partial(kernel, n_sp, n_dp, units_all, norm_scale, mix_scale),
        out_shape=(
            shape((seq_len, channels), BF16),
            shape((seq_len, channels), BF16),
            shape((piece, channels)),
            shape((GROUPS, BLK, BLK)),
            shape((GROUPS, BLK)),
            shape((1, channels)),
            shape((1, channels)),
        ),
        in_specs=[vmem] * 8,
        out_specs=(vmem,) * 7,
        scratch_shapes=[
            pltpu.VMEM((2 * n_sp, BLK // 2, depth), BF16),
            pltpu.VMEM((n_dp, piece, channels), BF16),
            pltpu.VMEM((seq_len, channels), F32),
            pltpu.VMEM((n_sp, 2, BLK), F32),
            pltpu.VMEM((n_sp, 2, BLK), F32),
            pltpu.VMEM((2, BLK), F32),
            pltpu.VMEM((n_sp, 2, BLK), F32),
            pltpu.VMEM((n_sp, 2, BLK), F32),
            pltpu.VMEM((n_sp, 2, BLK), F32),
            pltpu.VMEM((2, BLK), F32),
            pltpu.VMEM((n_sp, 2, BLK), F32),
            pltpu.VMEM(tile, BF16),
            pltpu.VMEM(tile, BF16),
            pltpu.VMEM(tile, F32),
            pltpu.VMEM((channels, depth), F32),
            pltpu.VMEM((seq_len, channels), F32),
            pltpu.VMEM((seq_len, channels), F32),
            pltpu.VMEM((seq_len, channels), F32),
            pltpu.VMEM(tile, F32),
            pltpu.VMEM(tile, F32),
            pltpu.VMEM(tile, F32),
            pltpu.VMEM(tile, F32),
            pltpu.VMEM((n_dp, 8, BLK), F32),
            pltpu.VMEM((n_dp, 8, BLK), F32),
            pltpu.VMEM((n_dp, piece, channels), BF16),
            pltpu.VMEM((n_dp, piece, channels), BF16),
            pltpu.VMEM((8, BLK), F32),
            pltpu.VMEM((n_sp, 8, BLK), F32),
            pltpu.VMEM((GROUPS * 8, BLK), BF16),
            pltpu.VMEM((n_dp, GROUPS * 8, BLK), BF16),
            dma((chunks,)), dma((chunks,)), dma((chunks,)), dma((chunks,)),
            dma((n_dp,)), dma((n_dp,)),
            dma((n_sp,)), dma((n_sp,)), dma((n_sp,)), dma((n_sp,)),
            dma((n_sp,)), dma((n_sp,)), dma((n_sp,)), dma((n_sp,)),
            dma((n_dp,)), dma((n_dp,)), dma((n_dp,)), dma((n_dp,)),
            dma((n_sp,)), dma((n_sp,)), dma((n_dp,)), dma((n_dp,)),
        ],
        compiler_params=pltpu.CompilerParams(
            collective_id=1, has_side_effects=True, vmem_limit_bytes=48 << 20
        ),
    )(
        cotangent.reshape(2, BLK // 2, depth),
        unit_pre[0],
        gate_pre[0],
        out_weight,
        mix_weight,
        mix_bias,
        norm_gain[None],
        norm_shift[None],
    )
    unit_grad, gate_grad, out_grad, weight_total, bias_total, gain_total, shift_total = outs
    return (
        unit_grad[None],
        gate_grad[None],
        out_grad,
        weight_total,
        bias_total,
        gain_total[0],
        shift_total[0],
    )


def solution(mesh):
    return jax.shard_map(
        local,
        mesh=mesh,
        in_specs=(
            P("dp", "sp", None),
            P("dp", None, "sp"),
            P("dp", None, "sp"),
            P("dp", "sp"),
            P(),
            P(),
            P("sp"),
            P("sp"),
        ),
        out_specs=(P("dp", None, "sp"), P("dp", None, "sp"), P("dp", "sp"), P(), P(), P("sp"), P("sp")),
        check_vma=False,
    )
```

time: 830 us -> 145 us (0.17)
  waiting for transfers between devices: 670 us -> 0 us
  Pallas kernels: 0 us -> 134 us
  starting transfers between devices: 53.6 us -> 0 us
  blocking collectives: 33.5 us -> 0 us
  matrix products: 18.9 us -> 0 us
  between operations: 14 us -> 0.68 us
  other arithmetic: 12.7 us -> 0 us
  local copies, waits for them, and re-layouts: 19.8 us -> 10.1 us
    psum x1 -> x0, waiting for transfers between devices: 430 us -> none  [local(): total = lax.psum(packed, ('sp', 'dp'))]
    pallas_call x0 -> x1, Pallas kernels: none -> 134 us  [local(): pl.pallas_call(functools.partial(kernel, n_sp, n_dp, units_all, norm_scal...]
    unnamed x4 -> x0, waiting for transfers between devices: 115 us -> none
    all_gather x1 -> x0, waiting for transfers between devices: 62.6 us -> none  [local(): weight_whole = lax.all_gather(weight_rows, 'dp', axis=0, tiled=True)]
    all_to_all x5 -> x0, waiting for transfers between devices: 62 us -> none  [the longest x1 22.5 us: local(): lax.all_to_all(head_rows.astype(jnp.bfloat16), 'sp', split_axis=1, concat...]
    all_to_all x5 -> x0, starting transfers between devices: 53.5 us -> none  [the longest x2 19.2 us: sum_over(): return lax.all_to_all(copies, axis, 0, 0, tiled=True).sum(axis=0)]
    all_gather x1 -> x0, blocking collectives: 33.5 us -> none  [local(): weight_rows = lax.all_gather(out_weight, 'sp', axis=1, tiled=True)]
    dot_general x5 -> x0, matrix products: 18.9 us -> none  [the longest x1 5.54 us: local(): lax.dot_general(cotangent[0], gated_rows, (((0,), (0,)), ((), ())), prefe...]
  transfers between devices with their start and end apart: 8 -> 0, of which waited for: 7 -> 0; matrix products, arithmetic and copies ran while one was open for 5% -> 0% of each run, Pallas kernels for 0% -> 0%
where the time goes in v3:
time: 145 us
  Pallas kernels  134 us (92%)
  local copies, waits for them, and re-layouts  10.1 us (7%)
    pallas_call x1, Pallas kernels, local(): pl.pallas_call(functools.partial(kernel, n_sp, n_dp, units_all, norm_scal...  134 us
    unnamed x23, local copies, waits for them, and re-layouts  10.1 us

profile of v3, /device:TPU:1, one launch (start us, length us, event | category | flops | bytes accessed | tf_op | source)
XLA Modules:
  0.0 145.1 jit_solution(14833977969604783755)
XLA Ops:
  0.6 0.0 copy-start.5
  0.6 0.0 copy-start.6
  0.7 0.0 copy-start.7
  0.7 0.7 copy-done.5
  1.3 0.0 copy-done.6
  1.3 0.0 copy-done.7
  1.3 0.0 copy-start
  1.3 1.0 copy-done
  2.4 0.0 copy-start.1
  2.4 1.0 copy-done.1
  3.4 0.0 copy-start.2
  3.4 1.0 copy-done.2
  4.5 0.0 copy-start.3
  4.5 0.9 copy-done.3
  5.4 0.0 copy-start.4
  5.4 0.7 copy-done.4
  6.1 134.4 %shard_map.135 = (bf16[2048,128]{1,0:T(8,128)(2,1)S(1)}, bf16[2048,128]{1,0:T(8,128)(2,1)S(1)}, f32[64,128]{1,0:T(8,128)S(1)}, f32[8,128,128]{2,1,0:T(8,128)S(1)...) custom-call(bf16[2,64,2048]{2,1,0:T(8,128)(2,1)S(1)} %bitcast.11, ...), custom_call_target="tpu_custom_call" | custom-call | tf_op jit(solution)/shard_map/pallas_call | solution.py:382
  140.5 0.8 copy.22
  141.3 0.8 copy.23
  142.1 0.6 copy.24
  142.7 0.8 copy.25
  143.5 0.6 copy.26
  144.1 0.5 copy.27
  144.6 0.5 copy.28
Async XLA Ops:
  0.6 0.7 copy-start.5
  0.6 0.7 copy-start.6
  0.7 0.7 copy-start.7
  1.3 1.0 copy-start
  2.4 1.0 copy-start.1
  3.4 1.0 copy-start.2
  4.5 0.9 copy-start.3
  5.4 0.7 copy-start.4

commit v4 on v3

--- a/solution.py
+++ b/solution.py
@@ -16,7 +16,10 @@
 
 epsilon = 1e-05
 tanh_coef = math.sqrt(2.0 / math.pi)
-SLABS = BLK // 8
+ROW = 8
+PART = BLK // ROW
+NEAR = 5
+GRANT = 65_390_000
 
 
 def gelu_pair(x):
@@ -53,19 +56,25 @@
 
 def kernel(
     n_sp, n_dp, units_all, norm_scale, mix_scale,
-    cot_ref, unit_ref, gate_ref, w_ref, mixw_ref, mixb_ref, gain_ref, shift_ref,
+    cot_hbm, unit_hbm, gate_hbm, w_hbm, mixw_hbm, mixb_hbm, gain_hbm, shift_hbm,
     ugrad_ref, ggrad_ref, dw_out, mix_out, bias_out, gain_out, shift_out,
     gbuf, w_all, gact_s, st_src, st_buf, st_own, st_all,
     bs_src, bs_buf, bs_own, bs_all, masked_s, masked_t, bias_s,
     dwt, scaled_s, cent_s, rs_s, mixacc, bacc, gacc, sacc,
     mix_src, m_buf, w_src, w_buf, b_own, b_buf, c_own, c_buf,
+    late_buf, g_src, g_buf, bias_own, bias_buf,
+    unit_ref, gate_ref, mixw_ref, mixb_ref, gain_ref, shift_ref, in_sem,
     r_send, r_recv, l_send, l_recv, wa_send, wa_recv,
     f1_send, f1_recv, f2_send, f2_recv, s1_send, s1_recv, s2_send, s2_recv,
     m_send, m_recv, w_send, w_recv, b_send, b_recv, c_send, c_recv,
+    late_send, late_recv, g_send, g_recv, bb_send, bb_recv,
 ):
     sp = lax.axis_index("sp")
     dp = lax.axis_index("dp")
-    depth = cot_ref.shape[2]
+    depth = cot_hbm.shape[2]
+    group = sp * GROUPS // n_sp
+    in_row = lax.rem(dp, ROW)
+    lates = n_sp - 1 - 2 * NEAR
     last = 2 * (n_sp // 2 - 1)
 
     def sp_at(d):
@@ -104,10 +113,21 @@
         return over_sp(bs_own, bs_all.at[sp], s2_send, s2_recv, d)
 
     def wa(d):
-        return over_dp(w_ref, w_all.at[dp], wa_send, wa_recv, d)
+        return over_dp(w_all.at[dp], w_all.at[dp], wa_send, wa_recv, d)
 
     def m1(d):
-        return over_dp(mix_src.at[dp_at(d)], m_buf.at[d], m_send, m_recv, d)
+        return over_dp(mix_src.at[lax.rem(dp_at(d), ROW)], m_buf.at[dp], m_send, m_recv, d)
+
+    def g1(d):
+        return over_dp(g_src, g_buf.at[dp], g_send, g_recv, d)
+
+    def bb1(d):
+        return over_sp(bias_own, bias_buf.at[sp], bb_send, bb_recv, d)
+
+    def late(d, k, p):
+        return pltpu.make_async_remote_copy(
+            bs_src.at[p], late_buf.at[k, sp], late_send.at[k, d], late_recv.at[k, d],
+            device_id={"sp": sp_at(d)}, device_id_type=MESH)
 
     def w1(d):
         return over_dp(w_src.at[dp_at(d)], w_buf.at[d], w_send, w_recv, d)
@@ -116,7 +136,10 @@
         return over_sp(b_own, b_buf.at[sp], b_send, b_recv, d)
 
     def c1(d):
-        return over_dp(c_own, c_buf.at[dp], c_send, c_recv, d)
+        peer = dp // ROW * ROW + lax.rem(in_row + d, ROW)
+        return pltpu.make_async_remote_copy(
+            c_own, c_buf.at[in_row], c_send.at[d], c_recv.at[d],
+            device_id={"dp": peer}, device_id_type=MESH)
 
     def to_right(src, at, c):
         return pltpu.make_async_remote_copy(
@@ -141,6 +164,27 @@
         barrier, inc=1, device_id={"sp": sp_at(d)}, device_id_type=MESH))
     each(n_dp, lambda d: pl.semaphore_signal(
         barrier, inc=1, device_id={"dp": dp_at(d)}, device_id_type=MESH))
+
+    loads = [
+        pltpu.make_async_copy(src, dst, in_sem.at[i])
+        for i, (src, dst) in enumerate(
+            [
+                (gate_hbm, gate_ref),
+                (cot_hbm, gbuf.at[pl.ds(2 * sp, 2)]),
+                (w_hbm, w_all.at[dp]),
+                (unit_hbm, unit_ref),
+                (mixw_hbm.at[group], mixw_ref),
+                (mixb_hbm, mixb_ref),
+                (gain_hbm, gain_ref),
+                (shift_hbm, shift_ref),
+            ]
+        )
+    ]
+    for load in loads:
+        load.start()
+    for acc in (mixacc, bacc, gacc, sacc, dwt):
+        acc[...] = jnp.zeros_like(acc)
+    loads[0].wait()
 
     def gate_sums(p, carry):
         rows = pl.ds(pl.multiple_of(p * BLK, BLK), BLK)
@@ -149,30 +193,33 @@
         st_src[p] = row_sums(act, act * act)
         return carry
 
+    def own_sends(c):
+        at = 2 * sp + c
+        back = 2 * sp + 1 - c
+        return to_right(gbuf.at[at], at, c), to_left(gbuf.at[back], back, c)
+
     lax.fori_loop(0, n_sp, gate_sums, 0)
+    loads[1].wait()
     pl.semaphore_wait(barrier, n_sp + n_dp - 2)
 
     each(n_sp, lambda d: f1(d).start())
     for c in range(2):
-        to_right(cot_ref.at[c], 2 * sp + c, c).start()
-        to_left(cot_ref.at[1 - c], 2 * sp + 1 - c, c).start()
+        for send in own_sends(c):
+            send.start()
+    loads[2].wait()
     each(n_dp, lambda d: wa(d).start())
-
-    for c in range(2):
-        gbuf[2 * sp + c] = cot_ref[c]
-    w_all[dp] = w_ref[...]
-    group = sp * GROUPS // n_sp
+    for load in loads[3:]:
+        load.wait()
+
     t_at = lax.broadcasted_iota(jnp.int32, (BLK, BLK), 0)
     s_at = lax.broadcasted_iota(jnp.int32, (BLK, BLK), 1)
     causal = t_at >= s_at
-    masked = jnp.where(causal, mixw_ref[group].astype(F32), 0.0)
+    masked = jnp.where(causal, mixw_ref[...].astype(F32), 0.0)
     masked_s[...] = masked.astype(BF16)
     masked_t[...] = jnp.transpose(masked).astype(BF16)
     picked = lax.broadcasted_iota(jnp.int32, (GROUPS, BLK), 0) == group
     bias_row = jnp.where(picked, mixb_ref[...].astype(F32), 0.0)
     bias_s[...] = dot(bias_row, jnp.ones((GROUPS, BLK), F32), 0, 0, lax.Precision.HIGHEST)
-    for acc in (mixacc, bacc, gacc, sacc, dwt, mix_src):
-        acc[...] = jnp.zeros_like(acc)
 
     each(n_sp, lambda d: f1(d).wait_recv())
     st_buf[0] = st_src[sp]
@@ -212,11 +259,18 @@
         scaled_s[rows, :] = scaled
         cent_s[rows, :] = centred
         rs_s[rows, :] = rstd * gate_slope
-        bs_src[p] = row_sums(scaled, scaled * centred)
-
-        @pl.when(b > 0)
+        sums = row_sums(scaled, scaled * centred)
+        bs_src[p] = sums
+
+        @pl.when(jnp.logical_and(b > 0, far <= NEAR))
         def _():
             s1(d).start()
+
+        @pl.when(far > NEAR)
+        def _():
+            k = d - NEAR - 1
+            late_buf[k, sp] = sums
+            each(n_sp, lambda e: late(e, k, p).start())
 
         return carry
 
@@ -241,6 +295,21 @@
         def _():
             each(n_sp, lambda d: f2(d).wait_recv())
             each(n_dp, lambda d: wa(d).wait_recv())
+
+        @pl.when(q == last)
+        def _():
+            def early(d):
+                @pl.when(jnp.logical_or(d <= NEAR, d >= n_sp - NEAR))
+                def _():
+                    s1(d).wait_recv()
+
+            each(n_sp, early)
+            own = bs_src[sp]
+            for d in range(1, NEAR + 1):
+                own = own + bs_buf[d] + bs_buf[n_sp - d]
+            bs_own[...] = own
+            bs_all[sp] = own
+            each(n_sp, lambda d: s2(d).start())
 
         @pl.when(q == last + 1)
         def _():
@@ -254,18 +323,24 @@
 
     lax.fori_loop(0, n_sp, step, 0)
 
-    mix_src[0:SLABS] = jnp.where(causal, mixacc[...], 0.0).reshape(SLABS, 8, BLK)
+    masked_grad = jnp.where(causal, mixacc[...], 0.0).astype(BF16)
+    for j in range(ROW):
+        mix_src[j] = masked_grad[j * PART : (j + 1) * PART]
+    each(n_dp, lambda d: m1(d).start())
     bias_sum = dot(jnp.ones((8, BLK), F32), bacc[...], 1, 1, lax.Precision.HIGHEST)[0:1]
-    mix_src[SLABS] = jnp.concatenate(
+    small = jnp.concatenate(
         [
             bias_sum,
             jnp.sum(gacc[...], axis=0, keepdims=True),
             jnp.sum(sacc[...], axis=0, keepdims=True),
-            jnp.zeros((5, BLK), F32),
+            jnp.zeros((1, BLK), F32),
         ],
         axis=0,
     )
-    each(n_dp, lambda d: m1(d).start())
+    g_src[...] = small
+    g_buf[dp] = small
+    m_buf[dp] = mix_src[in_row]
+    each(n_dp, lambda d: g1(d).start())
 
     piece = depth // n_dp
     per_tile = BLK // piece
@@ -275,70 +350,67 @@
         w_src[j * per_tile : (j + 1) * per_tile] = tile.reshape(per_tile, piece, BLK)
     each(n_dp, lambda d: w1(d).start())
 
-    each(n_sp, lambda d: s1(d).wait_recv())
-    bs_buf[0] = bs_src[sp]
-    back = jnp.sum(bs_buf[...], axis=0) * (1.0 / units_all)
-    bs_own[...] = back
-    bs_all[sp] = back
-    each(n_sp, lambda d: s2(d).start())
-
     each(n_dp, lambda d: m1(d).wait_recv())
-    m_buf[0] = mix_src[dp]
-    plane = jnp.sum(m_buf[...], axis=0)
+    plane = jnp.sum(m_buf[...].astype(F32), axis=0).astype(BF16)
     b_own[...] = plane
     b_buf[sp] = plane
-
-    @pl.when(dp <= SLABS)
-    def _():
-        each(n_sp, lambda d: b1(d).start())
+    each(n_sp, lambda d: b1(d).start())
+
+    each(n_dp, lambda d: g1(d).wait_recv())
+    plane_small = jnp.sum(g_buf[...], axis=0)
+    gain_out[...] = plane_small[1:2] * norm_scale
+    shift_out[...] = plane_small[2:3] * norm_scale
+    bias_own[...] = plane_small[0:1]
+    bias_buf[sp] = plane_small[0:1]
+    each(n_sp, lambda d: bb1(d).start())
 
     each(n_dp, lambda d: w1(d).wait_recv())
     w_buf[0] = w_src[dp]
     dw_out[...] = jnp.sum(w_buf[...].astype(F32), axis=0) * norm_scale
 
-    @pl.when(dp <= SLABS)
-    def _():
-        each(n_sp, lambda d: b1(d).wait_recv())
-        joined = jnp.sum(b_buf[...].reshape(GROUPS, n_sp // GROUPS, 8, BLK), axis=1)
-        at = lax.broadcasted_iota(jnp.int32, (GROUPS, 8, BLK), 1)
-        own = jnp.broadcast_to(b_own[...][None], (GROUPS, 8, BLK))
-        keep = jnp.logical_and(at >= 1, dp == SLABS)
-        sent = jnp.where(keep, own, joined).reshape(GROUPS * 8, BLK).astype(BF16)
-        c_own[...] = sent
-        c_buf[dp] = sent
-        each(n_dp, lambda d: c1(d).start())
-
     each(n_sp, lambda d: s2(d).wait_recv())
+    for k in range(lates):
+        each(n_sp, lambda d: late(d, k, sp_at(NEAR + 1 + k)).wait_recv())
 
     def gate_block(p, carry):
         rows = pl.ds(pl.multiple_of(p * BLK, BLK), BLK)
-        first_m, second_m = as_columns(bs_all[p])
+        total = bs_all[p]
+        for k in range(lates):
+            total = total + late_buf[k, lax.rem(p + n_sp - NEAR - 1 - k, n_sp)]
+        first_m, second_m = as_columns(total * (1.0 / units_all))
         inner = scaled_s[rows, :] - first_m - cent_s[rows, :] * second_m
         ggrad_ref[rows, :] = (inner * rs_s[rows, :]).astype(BF16)
         return carry
 
-    lax.fori_loop(0, n_sp, gate_block, 0)
-
-    def c_came(d):
-        @pl.when(dp_at(n_dp - d) <= SLABS)
-        def _():
-            c1(d).wait_recv()
-
-    each(n_dp, c_came)
-    for i in range(SLABS):
-        mix_out[:, 8 * i : 8 * i + 8, :] = (
-            c_buf[i].astype(F32).reshape(GROUPS, 8, BLK) * mix_scale
+    def gate_blocks(i, carry):
+        for k in range(4):
+            gate_block(4 * i + k, carry)
+        return carry
+
+    lax.fori_loop(0, n_sp // 4, gate_blocks, 0)
+
+    each(n_sp, lambda d: b1(d).wait_recv())
+    joined = jnp.sum(b_buf[...].astype(F32).reshape(GROUPS, n_sp // GROUPS, PART, BLK), axis=1)
+    sent = joined.reshape(GROUPS * PART, BLK).astype(BF16)
+    c_own[...] = sent
+    c_buf[in_row] = sent
+    each(ROW, lambda d: c1(d).start())
+
+    each(n_sp, lambda d: bb1(d).wait_recv())
+    per = n_sp // GROUPS
+    bias_out[...] = jnp.concatenate(
+        [sum(bias_buf[per * g + i] for i in range(per)) for g in range(GROUPS)], axis=0
+    ) * mix_scale
+
+    each(ROW, lambda d: c1(d).wait_recv())
+    for j in range(ROW):
+        mix_out[:, PART * j : PART * (j + 1), :] = (
+            c_buf[j].astype(F32).reshape(GROUPS, PART, BLK) * mix_scale
         )
-    small = c_buf[SLABS].astype(F32)
-    bias_out[...] = jnp.concatenate(
-        [small[8 * g : 8 * g + 1] for g in range(GROUPS)], axis=0
-    ) * mix_scale
-    gain_out[...] = small[1:2] * norm_scale
-    shift_out[...] = small[2:3] * norm_scale
 
     for c in range(2):
-        to_right(cot_ref.at[c], 2 * sp + c, c).wait_send()
-        to_left(cot_ref.at[1 - c], 2 * sp + 1 - c, c).wait_send()
+        for send in own_sends(c):
+            send.wait_send()
 
     def ring_sent(c, carry):
         at = came_right(c - 2)[0]
@@ -350,16 +422,34 @@
     lax.fori_loop(2, last + 1, ring_sent, 0)
     each(n_sp, lambda d: f1(d).wait_send())
     each(n_sp, lambda d: f2(d).wait_send())
-    each(n_sp, lambda d: s1(d).wait_send())
+
+    def early_sent(d):
+        @pl.when(jnp.logical_or(d <= NEAR, d >= n_sp - NEAR))
+        def _():
+            s1(d).wait_send()
+
+    each(n_sp, early_sent)
     each(n_sp, lambda d: s2(d).wait_send())
+    for k in range(lates):
+        each(n_sp, lambda d: late(d, k, sp_at(NEAR + 1 + k)).wait_send())
     each(n_dp, lambda d: wa(d).wait_send())
     each(n_dp, lambda d: m1(d).wait_send())
+    each(n_dp, lambda d: g1(d).wait_send())
     each(n_dp, lambda d: w1(d).wait_send())
-
-    @pl.when(dp <= SLABS)
-    def _():
-        each(n_sp, lambda d: b1(d).wait_send())
-        each(n_dp, lambda d: c1(d).wait_send())
+    each(n_sp, lambda d: b1(d).wait_send())
+    each(n_sp, lambda d: bb1(d).wait_send())
+    each(ROW, lambda d: c1(d).wait_send())
+
+
+def put_out(*refs):
+    count = len(refs) // 2
+    copies = [
+        pltpu.make_async_copy(refs[i], refs[count + i], refs[-1].at[i]) for i in range(count)
+    ]
+    for copy in copies:
+        copy.start()
+    for copy in copies:
+        copy.wait()
 
 
 def local(cotangent, unit_pre, gate_pre, out_weight, mix_weight, mix_bias, norm_gain, norm_shift):
@@ -372,6 +462,7 @@
     mix_scale = 1.0 / math.sqrt(token_count // BLK * (units_all // GROUPS))
     piece = depth // n_dp
     vmem = pl.BlockSpec(memory_space=pltpu.VMEM)
+    hbm = pl.BlockSpec(memory_space=pltpu.HBM)
     dma = pltpu.SemaphoreType.DMA
     tile = (BLK, BLK)
     chunks = n_sp - 1
@@ -379,18 +470,19 @@
     def shape(dims, dtype=F32):
         return jax.ShapeDtypeStruct(dims, dtype)
 
+    out_shapes = (
+        shape((seq_len, channels), BF16),
+        shape((seq_len, channels), BF16),
+        shape((piece, channels)),
+        shape((GROUPS, BLK, BLK)),
+        shape((GROUPS, BLK)),
+        shape((1, channels)),
+        shape((1, channels)),
+    )
     outs = pl.pallas_call(
         functools.partial(kernel, n_sp, n_dp, units_all, norm_scale, mix_scale),
-        out_shape=(
-            shape((seq_len, channels), BF16),
-            shape((seq_len, channels), BF16),
-            shape((piece, channels)),
-            shape((GROUPS, BLK, BLK)),
-            shape((GROUPS, BLK)),
-            shape((1, channels)),
-            shape((1, channels)),
-        ),
-        in_specs=[vmem] * 8,
+        out_shape=out_shapes,
+        in_specs=[hbm] * 8,
         out_specs=(vmem,) * 7,
         scratch_shapes=[
             pltpu.VMEM((2 * n_sp, BLK // 2, depth), BF16),
@@ -415,23 +507,37 @@
             pltpu.VMEM(tile, F32),
             pltpu.VMEM(tile, F32),
             pltpu.VMEM(tile, F32),
-            pltpu.VMEM((n_dp, 8, BLK), F32),
-            pltpu.VMEM((n_dp, 8, BLK), F32),
+            pltpu.VMEM((ROW, PART, BLK), BF16),
+            pltpu.VMEM((n_dp, PART, BLK), BF16),
             pltpu.VMEM((n_dp, piece, channels), BF16),
             pltpu.VMEM((n_dp, piece, channels), BF16),
-            pltpu.VMEM((8, BLK), F32),
-            pltpu.VMEM((n_sp, 8, BLK), F32),
-            pltpu.VMEM((GROUPS * 8, BLK), BF16),
-            pltpu.VMEM((n_dp, GROUPS * 8, BLK), BF16),
+            pltpu.VMEM((PART, BLK), BF16),
+            pltpu.VMEM((n_sp, PART, BLK), BF16),
+            pltpu.VMEM((GROUPS * PART, BLK), BF16),
+            pltpu.VMEM((ROW, GROUPS * PART, BLK), BF16),
+            pltpu.VMEM((n_sp - 1 - 2 * NEAR, n_sp, 2, BLK), F32),
+            pltpu.VMEM((4, BLK), F32),
+            pltpu.VMEM((n_dp, 4, BLK), F32),
+            pltpu.VMEM((1, BLK), F32),
+            pltpu.VMEM((n_sp, 1, BLK), F32),
+            pltpu.VMEM((seq_len, channels), BF16),
+            pltpu.VMEM((seq_len, channels), BF16),
+            pltpu.VMEM(tile, BF16),
+            pltpu.VMEM((GROUPS, BLK), BF16),
+            pltpu.VMEM((1, channels), BF16),
+            pltpu.VMEM((1, channels), BF16),
+            dma((8,)),
             dma((chunks,)), dma((chunks,)), dma((chunks,)), dma((chunks,)),
             dma((n_dp,)), dma((n_dp,)),
             dma((n_sp,)), dma((n_sp,)), dma((n_sp,)), dma((n_sp,)),
             dma((n_sp,)), dma((n_sp,)), dma((n_sp,)), dma((n_sp,)),
             dma((n_dp,)), dma((n_dp,)), dma((n_dp,)), dma((n_dp,)),
-            dma((n_sp,)), dma((n_sp,)), dma((n_dp,)), dma((n_dp,)),
+            dma((n_sp,)), dma((n_sp,)), dma((ROW,)), dma((ROW,)),
+            dma((n_sp - 1 - 2 * NEAR, n_sp)), dma((n_sp - 1 - 2 * NEAR, n_sp)),
+            dma((n_dp,)), dma((n_dp,)), dma((n_sp,)), dma((n_sp,)),
         ],
         compiler_params=pltpu.CompilerParams(
-            collective_id=1, has_side_effects=True, vmem_limit_bytes=48 << 20
+            collective_id=1, has_side_effects=True, vmem_limit_bytes=GRANT
         ),
     )(
         cotangent.reshape(2, BLK // 2, depth),
@@ -443,6 +549,14 @@
         norm_gain[None],
         norm_shift[None],
     )
+    outs = pl.pallas_call(
+        put_out,
+        out_shape=out_shapes,
+        in_specs=[vmem] * 7,
+        out_specs=(hbm,) * 7,
+        scratch_shapes=[dma((7,))],
+        compiler_params=pltpu.CompilerParams(vmem_limit_bytes=GRANT),
+    )(*outs)
     unit_grad, gate_grad, out_grad, weight_total, bias_total, gain_total, shift_total = outs
     return (
         unit_grad[None],

time: 145 us -> 140 us (0.966)
  local copies, waits for them, and re-layouts: 10.1 us -> 0 us
  Pallas kernels: 134 us -> 139 us
    unnamed x23 -> x0, local copies, waits for them, and re-layouts: 10.1 us -> none
    pallas_call x0 -> x1, Pallas kernels: none -> 2.59 us  [local(): pl.pallas_call(put_out, out_shape=out_shapes, in_specs=[vmem] * 7, out_sp...]
    pallas_call x1, Pallas kernels: 134 us -> 137 us  [local(): pl.pallas_call(functools.partial(kernel, n_sp, n_dp, units_all, norm_scal...]
where the time goes in v4:
time: 140 us
  Pallas kernels  139 us (99%)
    pallas_call x1, Pallas kernels, local(): pl.pallas_call(functools.partial(kernel, n_sp, n_dp, units_all, norm_scal...  137 us

profile of v4, /device:TPU:1, one launch (start us, length us, event | category | flops | bytes accessed | tf_op | source)
XLA Modules:
  0.0 139.9 jit_solution(4757821341498533677)
XLA Ops:
  0.6 136.7 %shard_map.135 = (bf16[2048,128]{1,0:T(8,128)(2,1)}, bf16[2048,128]{1,0:T(8,128)(2,1)}, f32[64,128]{1,0:T(8,128)}, f32[8,128,128]{2,1,0:T(8,128)}, f32[8,128]{1,...) custom-call(bf16[2,64,2048]{2,1,0:T(8,128)(2,1)} %bitcast.9, bf16[2048,128]{1,0:T(8,128)(2,1)} %bitcast.10, ...), custom_call_target="tpu_custom_call" | custom-call | tf_op jit(solution)/shard_map/pallas_call | solution.py:482
  137.3 2.6 %shard_map.136 = (bf16[2048,128]{1,0:T(8,128)(2,1)}, bf16[2048,128]{1,0:T(8,128)(2,1)}, f32[64,128]{1,0:T(8,128)}, f32[8,128,128]{2,1,0:T(8,128)}, f32[8,128]{1,...) custom-call(bf16[2048,128]{1,0:T(8,128)(2,1)} %get-tuple-element.21.refs_0_, ...), custom_call_target="tpu_custom_call" | custom-call | tf_op jit(solution)/shard_map/pallas_call | solution.py:552

commit v5 on v4

--- a/solution.py
+++ b/solution.py
@@ -17,8 +17,9 @@
 epsilon = 1e-05
 tanh_coef = math.sqrt(2.0 / math.pi)
 ROW = 8
+SIDE = 4
+FIRST = 4
 PART = BLK // ROW
-NEAR = 5
 GRANT = 65_390_000
 
 
@@ -62,19 +63,18 @@
     bs_src, bs_buf, bs_own, bs_all, masked_s, masked_t, bias_s,
     dwt, scaled_s, cent_s, rs_s, mixacc, bacc, gacc, sacc,
     mix_src, m_buf, w_src, w_buf, b_own, b_buf, c_own, c_buf,
-    late_buf, g_src, g_buf, bias_own, bias_buf,
+    g_src, g_buf, bias_own, bias_buf,
     unit_ref, gate_ref, mixw_ref, mixb_ref, gain_ref, shift_ref, in_sem,
     r_send, r_recv, l_send, l_recv, wa_send, wa_recv,
     f1_send, f1_recv, f2_send, f2_recv, s1_send, s1_recv, s2_send, s2_recv,
     m_send, m_recv, w_send, w_recv, b_send, b_recv, c_send, c_recv,
-    late_send, late_recv, g_send, g_recv, bb_send, bb_recv,
+    g_send, g_recv, bb_send, bb_recv, met,
 ):
     sp = lax.axis_index("sp")
     dp = lax.axis_index("dp")
     depth = cot_hbm.shape[2]
     group = sp * GROUPS // n_sp
     in_row = lax.rem(dp, ROW)
-    lates = n_sp - 1 - 2 * NEAR
     last = 2 * (n_sp // 2 - 1)
 
     def sp_at(d):
@@ -123,11 +123,6 @@
 
     def bb1(d):
         return over_sp(bias_own, bias_buf.at[sp], bb_send, bb_recv, d)
-
-    def late(d, k, p):
-        return pltpu.make_async_remote_copy(
-            bs_src.at[p], late_buf.at[k, sp], late_send.at[k, d], late_recv.at[k, d],
-            device_id={"sp": sp_at(d)}, device_id_type=MESH)
 
     def w1(d):
         return over_dp(w_src.at[dp_at(d)], w_buf.at[d], w_send, w_recv, d)
@@ -159,11 +154,26 @@
         at = 2 * sp_at(1 + c // 2) + 1 - lax.rem(c, 2)
         return at, to_left(gbuf.at[at], at, c)
 
+    core, x_at, y_at = lax.rem(dp, 2), lax.rem(dp // 2, SIDE), dp // (2 * SIDE)
+
+    def in_plane(dy, dx, dc):
+        line = lax.rem(y_at + dy, SIDE) * SIDE + lax.rem(x_at + dx, SIDE)
+        return {"dp": line * 2 + lax.rem(core + dc, 2)}
+
+    def greet(sem, peers):
+        for peer in peers:
+            pl.semaphore_signal(sem, inc=1, device_id=peer, device_id_type=MESH)
+
+    around = [in_plane(0, 0, 1), in_plane(0, 1, 0), in_plane(0, SIDE - 1, 0)]
+    around += [in_plane(1, 0, 0), in_plane(SIDE - 1, 0, 0), {"sp": right}, {"sp": left}]
+    across = [in_plane(0, 0, 1), in_plane(0, SIDE // 2, 0), in_plane(SIDE // 2, 0, 0)]
+    rounds = [
+        around,
+        across + [{"sp": sp_at(2)}, {"sp": sp_at(n_sp - 2)}],
+        across + [{"sp": sp_at(4)}, {"sp": sp_at(n_sp - 4)}],
+    ]
     barrier = pltpu.get_barrier_semaphore()
-    each(n_sp, lambda d: pl.semaphore_signal(
-        barrier, inc=1, device_id={"sp": sp_at(d)}, device_id_type=MESH))
-    each(n_dp, lambda d: pl.semaphore_signal(
-        barrier, inc=1, device_id={"dp": dp_at(d)}, device_id_type=MESH))
+    greet(barrier, around)
 
     loads = [
         pltpu.make_async_copy(src, dst, in_sem.at[i])
@@ -184,7 +194,6 @@
         load.start()
     for acc in (mixacc, bacc, gacc, sacc, dwt):
         acc[...] = jnp.zeros_like(acc)
-    loads[0].wait()
 
     def gate_sums(p, carry):
         rows = pl.ds(pl.multiple_of(p * BLK, BLK), BLK)
@@ -198,14 +207,19 @@
         back = 2 * sp + 1 - c
         return to_right(gbuf.at[at], at, c), to_left(gbuf.at[back], back, c)
 
-    lax.fori_loop(0, n_sp, gate_sums, 0)
     loads[1].wait()
-    pl.semaphore_wait(barrier, n_sp + n_dp - 2)
-
-    each(n_sp, lambda d: f1(d).start())
+    pl.semaphore_wait(barrier, len(around))
     for c in range(2):
         for send in own_sends(c):
             send.start()
+    loads[0].wait()
+    bounds = [0, n_sp // 2, n_sp, n_sp]
+    for r, peers in enumerate(rounds):
+        greet(met.at[r], peers)
+        lax.fori_loop(bounds[r], bounds[r + 1], gate_sums, 0)
+        pl.semaphore_wait(met.at[r], len(peers))
+
+    each(n_sp, lambda d: f1(d).start())
     loads[2].wait()
     each(n_dp, lambda d: wa(d).start())
     for load in loads[3:]:
@@ -259,18 +273,11 @@
         scaled_s[rows, :] = scaled
         cent_s[rows, :] = centred
         rs_s[rows, :] = rstd * gate_slope
-        sums = row_sums(scaled, scaled * centred)
-        bs_src[p] = sums
-
-        @pl.when(jnp.logical_and(b > 0, far <= NEAR))
+        bs_src[p] = row_sums(scaled, scaled * centred)
+
+        @pl.when(b > 0)
         def _():
             s1(d).start()
-
-        @pl.when(far > NEAR)
-        def _():
-            k = d - NEAR - 1
-            late_buf[k, sp] = sums
-            each(n_sp, lambda e: late(e, k, p).start())
 
         return carry
 
@@ -291,33 +298,18 @@
             def _():
                 to_left(gbuf.at[at_left], at_left, q + 2).start()
 
-        @pl.when(q == 2)
+        @pl.when(q == FIRST)
         def _():
             each(n_sp, lambda d: f2(d).wait_recv())
             each(n_dp, lambda d: wa(d).wait_recv())
-
-        @pl.when(q == last)
-        def _():
-            def early(d):
-                @pl.when(jnp.logical_or(d <= NEAR, d >= n_sp - NEAR))
-                def _():
-                    s1(d).wait_recv()
-
-            each(n_sp, early)
-            own = bs_src[sp]
-            for d in range(1, NEAR + 1):
-                own = own + bs_buf[d] + bs_buf[n_sp - d]
-            bs_own[...] = own
-            bs_all[sp] = own
-            each(n_sp, lambda d: s2(d).start())
 
         @pl.when(q == last + 1)
         def _():
             came_right(last)[1].wait_recv()
             came_left(last)[1].wait_recv()
 
-        lo = jnp.maximum(0, jnp.minimum(2 * (q - 2), q))
-        hi = jnp.maximum(0, jnp.minimum(2 * (q - 2) + 2, q + 1))
+        lo = jnp.maximum(0, jnp.minimum(2 * (q - FIRST), q))
+        hi = jnp.maximum(0, jnp.minimum(2 * (q - FIRST) + 2, q + 1))
         lax.fori_loop(lo, hi, block, 0)
         return carry
 
@@ -356,6 +348,13 @@
     b_buf[sp] = plane
     each(n_sp, lambda d: b1(d).start())
 
+    each(n_sp, lambda d: s1(d).wait_recv())
+    bs_buf[0] = bs_src[sp]
+    back = jnp.sum(bs_buf[...], axis=0) * (1.0 / units_all)
+    bs_own[...] = back
+    bs_all[sp] = back
+    each(n_sp, lambda d: s2(d).start())
+
     each(n_dp, lambda d: g1(d).wait_recv())
     plane_small = jnp.sum(g_buf[...], axis=0)
     gain_out[...] = plane_small[1:2] * norm_scale
@@ -368,27 +367,6 @@
     w_buf[0] = w_src[dp]
     dw_out[...] = jnp.sum(w_buf[...].astype(F32), axis=0) * norm_scale
 
-    each(n_sp, lambda d: s2(d).wait_recv())
-    for k in range(lates):
-        each(n_sp, lambda d: late(d, k, sp_at(NEAR + 1 + k)).wait_recv())
-
-    def gate_block(p, carry):
-        rows = pl.ds(pl.multiple_of(p * BLK, BLK), BLK)
-        total = bs_all[p]
-        for k in range(lates):
-            total = total + late_buf[k, lax.rem(p + n_sp - NEAR - 1 - k, n_sp)]
-        first_m, second_m = as_columns(total * (1.0 / units_all))
-        inner = scaled_s[rows, :] - first_m - cent_s[rows, :] * second_m
-        ggrad_ref[rows, :] = (inner * rs_s[rows, :]).astype(BF16)
-        return carry
-
-    def gate_blocks(i, carry):
-        for k in range(4):
-            gate_block(4 * i + k, carry)
-        return carry
-
-    lax.fori_loop(0, n_sp // 4, gate_blocks, 0)
-
     each(n_sp, lambda d: b1(d).wait_recv())
     joined = jnp.sum(b_buf[...].astype(F32).reshape(GROUPS, n_sp // GROUPS, PART, BLK), axis=1)
     sent = joined.reshape(GROUPS * PART, BLK).astype(BF16)
@@ -396,6 +374,21 @@
     c_buf[in_row] = sent
     each(ROW, lambda d: c1(d).start())
 
+    each(n_sp, lambda d: s2(d).wait_recv())
+
+    def gate_block(p):
+        rows = pl.ds(pl.multiple_of(p * BLK, BLK), BLK)
+        first_m, second_m = as_columns(bs_all[p])
+        inner = scaled_s[rows, :] - first_m - cent_s[rows, :] * second_m
+        ggrad_ref[rows, :] = (inner * rs_s[rows, :]).astype(BF16)
+
+    def gate_blocks(i, carry):
+        for k in range(4):
+            gate_block(4 * i + k)
+        return carry
+
+    lax.fori_loop(0, n_sp // 4, gate_blocks, 0)
+
     each(n_sp, lambda d: bb1(d).wait_recv())
     per = n_sp // GROUPS
     bias_out[...] = jnp.concatenate(
@@ -423,15 +416,8 @@
     each(n_sp, lambda d: f1(d).wait_send())
     each(n_sp, lambda d: f2(d).wait_send())
 
-    def early_sent(d):
-        @pl.when(jnp.logical_or(d <= NEAR, d >= n_sp - NEAR))
-        def _():
-            s1(d).wait_send()
-
-    each(n_sp, early_sent)
+    each(n_sp, lambda d: s1(d).wait_send())
     each(n_sp, lambda d: s2(d).wait_send())
-    for k in range(lates):
-        each(n_sp, lambda d: late(d, k, sp_at(NEAR + 1 + k)).wait_send())
     each(n_dp, lambda d: wa(d).wait_send())
     each(n_dp, lambda d: m1(d).wait_send())
     each(n_dp, lambda d: g1(d).wait_send())
@@ -515,7 +501,6 @@
             pltpu.VMEM((n_sp, PART, BLK), BF16),
             pltpu.VMEM((GROUPS * PART, BLK), BF16),
             pltpu.VMEM((ROW, GROUPS * PART, BLK), BF16),
-            pltpu.VMEM((n_sp - 1 - 2 * NEAR, n_sp, 2, BLK), F32),
             pltpu.VMEM((4, BLK), F32),
             pltpu.VMEM((n_dp, 4, BLK), F32),
             pltpu.VMEM((1, BLK), F32),
@@ -533,8 +518,8 @@
             dma((n_sp,)), dma((n_sp,)), dma((n_sp,)), dma((n_sp,)),
             dma((n_dp,)), dma((n_dp,)), dma((n_dp,)), dma((n_dp,)),
             dma((n_sp,)), dma((n_sp,)), dma((ROW,)), dma((ROW,)),
-            dma((n_sp - 1 - 2 * NEAR, n_sp)), dma((n_sp - 1 - 2 * NEAR, n_sp)),
             dma((n_dp,)), dma((n_dp,)), dma((n_sp,)), dma((n_sp,)),
+            pltpu.SemaphoreType.REGULAR((3,)),
         ],
         compiler_params=pltpu.CompilerParams(
             collective_id=1, has_side_effects=True, vmem_limit_bytes=GRANT

time: 140 us -> 137 us (0.979)
  Pallas kernels: 139 us -> 136 us
    pallas_call x1, Pallas kernels: 137 us -> 133 us  [local(): pl.pallas_call(functools.partial(kernel, n_sp, n_dp, units_all, norm_scal...]
where the time goes in v5:
time: 137 us
  Pallas kernels  136 us (99%)
    pallas_call x1, Pallas kernels, local(): pl.pallas_call(functools.partial(kernel, n_sp, n_dp, units_all, norm_scal...  133 us

profile of v5, /device:TPU:1, one launch (start us, length us, event | category | flops | bytes accessed | tf_op | source)
XLA Modules:
  0.0 136.6 jit_solution(742116975188060102)
XLA Ops:
  0.6 133.4 %shard_map.135 = (bf16[2048,128]{1,0:T(8,128)(2,1)}, bf16[2048,128]{1,0:T(8,128)(2,1)}, f32[64,128]{1,0:T(8,128)}, f32[8,128,128]{2,1,0:T(8,128)}, f32[8,128]{1,...) custom-call(bf16[2,64,2048]{2,1,0:T(8,128)(2,1)} %bitcast.9, bf16[2048,128]{1,0:T(8,128)(2,1)} %bitcast.10, ...), custom_call_target="tpu_custom_call" | custom-call | tf_op jit(solution)/shard_map/pallas_call | solution.py:468
  134.0 2.6 %shard_map.136 = (bf16[2048,128]{1,0:T(8,128)(2,1)}, bf16[2048,128]{1,0:T(8,128)(2,1)}, f32[64,128]{1,0:T(8,128)}, f32[8,128,128]{2,1,0:T(8,128)}, f32[8,128]{1,...) custom-call(bf16[2048,128]{1,0:T(8,128)(2,1)} %get-tuple-element.21.refs_0_, ...), custom_call_target="tpu_custom_call" | custom-call | tf_op jit(solution)/shard_map/pallas_call | solution.py:537

commit v6 on v5

--- a/solution.py
+++ b/solution.py
@@ -18,7 +18,8 @@
 tanh_coef = math.sqrt(2.0 / math.pi)
 ROW = 8
 SIDE = 4
-FIRST = 4
+SUMS = 2
+FIRST = 6
 PART = BLK // ROW
 GRANT = 65_390_000
 
@@ -234,16 +235,6 @@
     picked = lax.broadcasted_iota(jnp.int32, (GROUPS, BLK), 0) == group
     bias_row = jnp.where(picked, mixb_ref[...].astype(F32), 0.0)
     bias_s[...] = dot(bias_row, jnp.ones((GROUPS, BLK), F32), 0, 0, lax.Precision.HIGHEST)
-
-    each(n_sp, lambda d: f1(d).wait_recv())
-    st_buf[0] = st_src[sp]
-    moments = jnp.sum(st_buf[...], axis=0) * (1.0 / units_all)
-    mean_row = moments[0:1]
-    rstd_row = lax.rsqrt(moments[1:2] - mean_row * mean_row + epsilon)
-    norm_row = jnp.concatenate([mean_row, rstd_row], axis=0)
-    st_own[...] = norm_row
-    st_all[sp] = norm_row
-    each(n_sp, lambda d: f2(d).start())
 
     def block(b, carry):
         far = (b + 1) // 2
@@ -297,6 +288,18 @@
             @pl.when(q < last - 1)
             def _():
                 to_left(gbuf.at[at_left], at_left, q + 2).start()
+
+        @pl.when(q == SUMS)
+        def _():
+            each(n_sp, lambda d: f1(d).wait_recv())
+            st_buf[0] = st_src[sp]
+            moments = jnp.sum(st_buf[...], axis=0) * (1.0 / units_all)
+            mean_row = moments[0:1]
+            rstd_row = lax.rsqrt(moments[1:2] - mean_row * mean_row + epsilon)
+            norm_row = jnp.concatenate([mean_row, rstd_row], axis=0)
+            st_own[...] = norm_row
+            st_all[sp] = norm_row
+            each(n_sp, lambda d: f2(d).start())
 
         @pl.when(q == FIRST)
         def _():

time: 137 us -> 136 us (level)
  no operation moved by 1% of the time
where the time goes in v6:
time: 136 us; the launch traced here: 135 us
  Pallas kernels  135 us (99%)
    pallas_call x1, Pallas kernels, local(): pl.pallas_call(functools.partial(kernel, n_sp, n_dp, units_all, norm_scal...  132 us

profile of v6, /device:TPU:1, one launch (start us, length us, event | category | flops | bytes accessed | tf_op | source)
XLA Modules:
  0.0 135.4 jit_solution(4719780147240405844)
XLA Ops:
  0.6 132.1 %shard_map.135 = (bf16[2048,128]{1,0:T(8,128)(2,1)}, bf16[2048,128]{1,0:T(8,128)(2,1)}, f32[64,128]{1,0:T(8,128)}, f32[8,128,128]{2,1,0:T(8,128)}, f32[8,128]{1,...) custom-call(bf16[2,64,2048]{2,1,0:T(8,128)(2,1)} %bitcast.9, bf16[2048,128]{1,0:T(8,128)(2,1)} %bitcast.10, ...), custom_call_target="tpu_custom_call" | custom-call | tf_op jit(solution)/shard_map/pallas_call | solution.py:471
  132.8 2.6 %shard_map.136 = (bf16[2048,128]{1,0:T(8,128)(2,1)}, bf16[2048,128]{1,0:T(8,128)(2,1)}, f32[64,128]{1,0:T(8,128)}, f32[8,128,128]{2,1,0:T(8,128)}, f32[8,128]{1,...) custom-call(bf16[2048,128]{1,0:T(8,128)(2,1)} %get-tuple-element.21.refs_0_, ...), custom_call_target="tpu_custom_call" | custom-call | tf_op jit(solution)/shard_map/pallas_call | solution.py:540
